TPU v7x, 128 devices: a whole 4x4x4 slice. The times are simulated.
128 devices in a mesh: dp: 4 (over x), kv: 16 (over z, y), tp: 2 (over core).
Axes of the slice: x: 4, y: 4, z: 4, core: 2. Of those that a mesh axis runs over, the one named last changes fastest.
Arguments:
- tokens: bfloat16 [8192, 2048], P('dp', 'kv'), may hold values from -70 to 70
- pre_gain: float32 [2048], replicated, may hold values from 0.1 to 1.9
- query_weight: bfloat16 [2048, 1024], P(None, 'tp'), may hold values from -0.125 to 0.125
- key_weight: bfloat16 [2048, 1024], P(None, 'tp'), may hold values from -0.125 to 0.125
- value_weight: bfloat16 [2048, 1024], P(None, 'tp'), may hold values from -0.125 to 0.125
- gate_weight: bfloat16 [2048, 1024], P(None, 'tp'), may hold values from -0.125 to 0.125
- beta_weight: bfloat16 [2048, 8], replicated, may hold values from -0.125 to 0.125
- decay_weight: bfloat16 [2048, 8], replicated, may hold values from -0.125 to 0.125
- decay_log: float32 [8], P('tp'), may hold values from -3 to 0.5
- head_gain: float32 [128], replicated, may hold values from 0.1 to 1.9
- out_weight: bfloat16 [1024, 2048], P('tp', 'kv'), may hold values from -1 to 1
- post_gain: float32 [2048], P(('kv', 'tp')), may hold values from 0.1 to 1.9
- saved_state: float32 [2048, 8, 128, 128], P(('dp', 'kv'), 'tp'), may hold values from -4 to 4
- earlier_keys: bfloat16 [2048, 4, 8, 128], P(('dp', 'kv'), None, 'tp'), may hold values from -6 to 6
- earlier_values: bfloat16 [2048, 4, 8, 128], P(('dp', 'kv'), None, 'tp'), may hold values from -6 to 6
- earlier_rates: float32 [2048, 4, 8], P(('dp', 'kv'), None, 'tp'), may hold values from 0.05 to 0.95
- earlier_decays: float32 [2048, 4, 8], P(('dp', 'kv'), None, 'tp'), may hold values from -1.5 to -0.02
- accepted: int32 [2048], P(('dp', 'kv')), may hold values from 0 to 4
Outputs:
- mixed: bfloat16 [8192, 2048], P('dp', ('kv', 'tp'))
- committed: float32 [2048, 8, 128, 128], P(('dp', 'kv'), 'tp')
All inputs are finite; a program needn't handle non-finite values.
Results may differ from a plain program's by a relative error of at most 0.011.
Values may be sent and summed in bfloat16 or wider, within the bound.
No kernel may reach another device: no remote copies, remote signals or barrier semaphores. Data moves between devices by JAX's collectives and lax.ppermute only.
A program may use at most 128 MiB of HBM per device.

v0:
```python
import jax
import jax.numpy as jnp
from jax import lax
from jax.sharding import PartitionSpec as P


def in_order(tiles, dim):
    dims = list(tiles.shape[1:])
    dims[dim] *= tiles.shape[0]
    return jnp.moveaxis(tiles, 0, dim).reshape(dims)


def from_everyone(shard, axis):
    count = lax.axis_size(axis)
    return lax.all_to_all(
        jnp.broadcast_to(shard[None], (count, *shard.shape)), axis, 0, 0, tiled=True
    )


def collect(shard, axis, dim):
    return in_order(from_everyone(shard, axis), dim)


def cut_along(shard, dim, count):
    before, after = (shard.shape[:dim], shard.shape[dim + 1 :])
    return jnp.moveaxis(shard.reshape(*before, count, -1, *after), dim, 0)


def summed_on_arrival(shard, axis, dim):
    count = lax.axis_size(axis)
    tiles = lax.all_to_all(cut_along(shard, dim, count), axis, 0, 0, tiled=True)
    return jnp.sum(tiles.astype(jnp.float32), axis=0)


def taken_together(shard, axis):
    everything = from_everyone(shard, axis)
    return jnp.sum(everything, axis=0)


def unit_norm(values):
    return values * lax.rsqrt(jnp.sum(values * values, axis=-1, keepdims=True) + 1e-06)


def advance(current, key_row, value_row, rate_now, log_decay):
    recalled = jnp.sum(key_row[..., :, None] * current, axis=-2)
    rate_cube = rate_now[..., None, None]
    current = current - rate_cube * key_row[..., :, None] * recalled[..., None, :]
    return (
        jnp.exp(log_decay)[..., None, None] * current
        + rate_cube * key_row[..., :, None] * value_row[..., None, :]
    )


def run_heads(
    saved_state,
    earlier_keys,
    earlier_values,
    earlier_rates,
    earlier_decays,
    accepted,
    queries,
    keys_unit,
    values_act,
    rates,
    decays,
):
    current = saved_state
    proposals = earlier_keys.shape[1]
    for position in range(proposals):
        live = (position < accepted).astype(jnp.float32)
        live = live.reshape(live.shape + (1,) * (earlier_rates.ndim - 2))
        current = advance(
            current,
            earlier_keys[:, position],
            earlier_values[:, position],
            earlier_rates[:, position] * live,
            earlier_decays[:, position] * live,
        )
    committed = current
    outputs = []
    for position in range(proposals):
        current = advance(
            current,
            keys_unit[:, position],
            values_act[:, position],
            rates[:, position],
            decays[:, position],
        )
        outputs.append(jnp.sum(queries[:, position][..., :, None] * current, axis=-2))
    return (committed, jnp.stack(outputs, axis=1))


def local(
    tokens,
    pre_gain,
    query_weight,
    key_weight,
    value_weight,
    gate_weight,
    beta_weight,
    decay_weight,
    decay_log,
    head_gain,
    out_weight,
    post_gain,
    saved_state,
    earlier_keys,
    earlier_values,
    earlier_rates,
    earlier_decays,
    accepted,
):
    seq_local = saved_state.shape[0]
    heads_local = saved_state.shape[1]
    head_size = saved_state.shape[2]
    proposals = earlier_keys.shape[1]
    rows_local = seq_local * proposals
    width_local = heads_local * head_size
    model_width = pre_gain.shape[0]
    head_start = lax.axis_index("tp") * heads_local
    beta_cols = lax.dynamic_slice_in_dim(beta_weight, head_start, heads_local, 1)
    decay_cols = lax.dynamic_slice_in_dim(decay_weight, head_start, heads_local, 1)
    own_rows = lax.all_to_all(tokens, "kv", split_axis=0, concat_axis=1, tiled=True)
    widened = own_rows.astype(jnp.float32)
    inverse = lax.rsqrt(jnp.mean(widened * widened, axis=1) + 1e-06)
    scaled = (widened * pre_gain).astype(jnp.bfloat16)
    stacked = jnp.stack(
        [
            jnp.dot(scaled, weight, preferred_element_type=jnp.float32)
            for weight in (query_weight, key_weight, value_weight, gate_weight)
        ],
        axis=1,
    )
    scalars = jnp.stack(
        [
            jnp.dot(scaled, cols, preferred_element_type=jnp.float32)
            for cols in (beta_cols, decay_cols)
        ],
        axis=1,
    )
    stacked = stacked * inverse[:, None, None]
    scalars = scalars * inverse[:, None, None]

    def heads_of(values):
        return values.reshape(seq_local, proposals, heads_local, head_size)

    queries = unit_norm(jax.nn.silu(heads_of(stacked[:, 0]))) * head_size ** (-0.5)
    keys_unit = unit_norm(jax.nn.silu(heads_of(stacked[:, 1])))
    values_act = jax.nn.silu(heads_of(stacked[:, 2]))
    gates_raw = heads_of(stacked[:, 3])
    rates = jax.nn.sigmoid(scalars[:, 0]).reshape(seq_local, proposals, heads_local)
    decays = -jnp.exp(decay_log) * jax.nn.softplus(scalars[:, 1]).reshape(
        seq_local, proposals, heads_local
    )
    committed, reads = run_heads(
        saved_state,
        unit_norm(earlier_keys.astype(jnp.float32)),
        earlier_values.astype(jnp.float32),
        earlier_rates,
        earlier_decays,
        accepted,
        queries,
        keys_unit,
        values_act,
        rates,
        decays,
    )
    normed = reads * lax.rsqrt(jnp.mean(reads * reads, axis=-1, keepdims=True) + 1e-06) * head_gain
    attended = (
        (normed * jax.nn.silu(gates_raw)).reshape(rows_local, width_local).astype(jnp.bfloat16)
    )
    partial_value = jnp.dot(
        collect(attended, "kv", 0), out_weight, preferred_element_type=jnp.float32
    )
    column_part = summed_on_arrival(partial_value.astype(jnp.bfloat16), "tp", 1)
    totals = taken_together(jnp.sum(column_part * column_part, axis=1), ("kv", "tp"))
    factor = lax.rsqrt(totals / model_width + 1e-06)
    mixed = (column_part * factor[:, None] * post_gain).astype(jnp.bfloat16)
    return (mixed, committed)


def solution(mesh):
    placed = (
        P("dp", "kv"),
        P(),
        P(None, "tp"),
        P(None, "tp"),
        P(None, "tp"),
        P(None, "tp"),
        P(),
        P(),
        P("tp"),
        P(),
        P("tp", "kv"),
        P(("kv", "tp")),
        P(("dp", "kv"), "tp", None, None),
        P(("dp", "kv"), None, "tp", None),
        P(("dp", "kv"), None, "tp", None),
        P(("dp", "kv"), None, "tp"),
        P(("dp", "kv"), None, "tp"),
        P(("dp", "kv")),
    )
    return jax.shard_map(
        local,
        mesh=mesh,
        in_specs=placed,
        out_specs=(P("dp", ("kv", "tp")), P(("dp", "kv"), "tp", None, None)),
        check_vma=False,
    )
```

profile of v0, /device:TPU:1, one launch (start us, length us, event | category | flops | bytes accessed | tf_op | source)
XLA Modules:
  0.0 188.4 jit_solution(10314389959742774240)
XLA Ops:
  0.6 8.7 %all-to-all-start = ((bf16[16,128,128]{2,1,0:T(8,128)(2,1)}), bf16[16,128,128]{2,1,0:T(8,128)(2,1)S(1)}, u32[]{:S(2)}, u32[]{:S(2)}) async-start(bf16[16,128,128]{2,1,0:T(8,128)(2,1)} %bitcast.154), calls=%async_computation | async-start | bytes 1048576 | tf_op jit(solution)/shard_map/all_to_all | solution.py:123
  9.4 0.7 exponential_negate_fusion
  10.1 1.2 broadcast_bitcast_fusion
  11.3 0.7 compare_convert_fusion.3
  12.0 0.8 bitcast_multiply_fusion.2
  12.8 0.1 copy.104
  13.5 1.1 fusion.40
  14.6 1.1 convert_multiply_fusion.1
  15.7 0.9 convert_element_type.60
  16.7 0.1 slice_bitcast_fusion.12
  16.8 0.2 broadcast_multiply_fusion.6
  17.0 9.6 %multiply_add_fusion.6 = f32[32,4,128,128]{3,2,1,0:T(8,128)S(1)} fusion(f32[32,4,128,128]{3,2,1,0:T(8,128)} %param.30, f32[32,4,128]{2,1,0:T(4,128)S(1)} %get-tuple-element.34, f32[32,4,128]{2,1,0:T(4,128)S(1)} %get-tuple-element.30, f32[32,4]{1,0:T(8,128)S(1)} %copy.100, f32[32,4,128]{2,1,0:T(4,128)S(1)} %get-tuple-element.65), kind=kOutput, calls=%fused_computation.32 | output fusion | flops 12599423 | bytes 16974336 | tf_op jit(solution)/shard_map/mul | solution.py:47
  26.6 15.4 %multiply_add_fusion.5 = f32[32,4,128,128]{3,2,1,0:T(8,128)S(1)} fusion(f32[32,4,128,128]{3,2,1,0:T(8,128)S(1)} %multiply_add_fusion.6, f32[32,4,128]{2,1,0:T(4,128)S(1)} %get-tuple-element.33, f32[32,4,128]{2,1,0:T(4,128)S(1)} %get-tuple-element.29, f32[32,4]{1,0:T(8,128)S(1)} %copy.99, f32[32,4,128]{2,1,0:T(4,128)S(1)} %get-tuple-element.66), kind=kOutput, calls=%fused_computation.29 | output fusion | flops 12599423 | bytes 16974336 | tf_op jit(solution)/shard_map/mul | solution.py:47
  42.0 15.4 %multiply_add_fusion.4 = f32[32,4,128,128]{3,2,1,0:T(8,128)S(1)} fusion(f32[32,4,128,128]{3,2,1,0:T(8,128)S(1)} %multiply_add_fusion.5, f32[32,4,128]{2,1,0:T(4,128)S(1)} %get-tuple-element.32, f32[32,4,128]{2,1,0:T(4,128)S(1)} %get-tuple-element.28, f32[32,4]{1,0:T(8,128)S(1)} %copy.98, f32[32,4,128]{2,1,0:T(4,128)S(1)} %get-tuple-element.67), kind=kOutput, calls=%fused_computation.26 | output fusion | flops 12599423 | bytes 16974336 | tf_op jit(solution)/shard_map/mul | solution.py:47
  57.5 7.1 %multiply_add_fusion.3 = f32[32,4,128,128]{3,2,1,0:T(8,128)} fusion(f32[32,4,128,128]{3,2,1,0:T(8,128)S(1)} %multiply_add_fusion.4, f32[32,4,128]{2,1,0:T(4,128)S(1)} %get-tuple-element.31, f32[32,4,128]{2,1,0:T(4,128)S(1)} %get-tuple-element.27, f32[32,4]{1,0:T(8,128)S(1)} %copy.97, f32[32,4,128]{2,1,0:T(4,128)S(1)} %get-tuple-element.68), kind=kOutput, calls=%fused_computation.23 | output fusion | flops 12599423 | bytes 16974336 | tf_op jit(solution)/shard_map/mul | solution.py:47
  64.6 0.2 fusion.38
  64.8 1.1 convert_bitcast_fusion
  65.9 2.6 %copy.95 = f32[128,16,128]{0,2,1:T(8,128)} copy(f32[128,16,128]{2,0,1:T(8,128)} %convert_bitcast_fusion) | data formatting | bytes 2097152 | tf_op jit(solution)/shard_map/convert_element_type | solution.py:124
  68.5 1.6 fusion.39
  70.1 0.2 convolution_bitcast_fusion.4
  70.3 0.2 convolution_bitcast_fusion.5
  70.5 0.1 squeeze.32
  70.6 0.1 div.55
  70.7 0.1 fusion.61
  70.8 0.3 copy.120
  71.1 0.3 copy.118
  71.4 0.3 copy.116
  71.7 0.3 copy.114
  72.1 0.1 slice_exponential_fusion
  72.3 0.3 copy.119
  72.6 0.9 copy.117
  73.4 0.9 copy.115
  74.3 0.9 copy.113
  75.2 0.5 convolution_bitcast_fusion
  75.7 2.2 %convolution_bitcast_fusion.1 = f32[128,1,512]{2,0,1:T(8,128)S(1)} fusion(bf16[128,2048]{0,1:T(8,128)(2,1)S(1)} %fusion.39, bf16[2048,512]{1,0:T(8,128)(2,1)} %param.22), kind=kOutput, calls=%fused_computation.47 | convolution fusion | flops 268435456 | bytes 2883584 | tf_op jit(solution)/shard_map/dot_general | solution.py:129
  77.9 2.1 %convolution_bitcast_fusion.2 = f32[128,1,512]{2,0,1:T(8,128)S(1)} fusion(bf16[128,2048]{0,1:T(8,128)(2,1)S(1)} %fusion.39, bf16[2048,512]{1,0:T(8,128)(2,1)} %param.21), kind=kOutput, calls=%fused_computation.48 | convolution fusion | flops 268435456 | bytes 2883584 | tf_op jit(solution)/shard_map/dot_general | solution.py:129
  80.0 0.5 convolution_bitcast_fusion.3
  80.5 0.1 maximum_multiply_fusion
  80.7 0.1 reshape_squeeze.12
  80.8 0.3 multiply_reduce_fusion.15
  81.1 0.2 multiply_multiply_fusion
  81.3 0.7 slice_bitcast_fusion.20
  82.0 0.1 reshape_squeeze.13
  82.1 0.3 multiply_reduce_fusion.14
  82.4 0.2 broadcast_multiply_fusion.1
  82.6 0.1 reshape_squeeze.14
  82.7 0.1 divide_multiply_fusion
  82.9 0.1 slice_bitcast_fusion.1
  83.0 0.2 broadcast_multiply_fusion.2
  83.2 12.4 %multiply_reduce_fusion.6 = (f32[32,4,128]{2,1,0:T(4,128)S(1)}, f32[32,4,128,128]{3,2,1,0:T(8,128)S(1)}) fusion(f32[32,4,128]{2,1,0:T(4,128)S(1)} %get-tuple-element.7, f32[32,4,128]{2,1,0:T(4,128)S(1)} %get-tuple-element.22, f32[32,4,128,128]{3,2,1,0:T(8,128)} %multiply_add_fusion.3, f32[32,4,128]{2,1,0:T(4,128)S(1)} %get-tuple-element.69, ...), kind=kOutput, calls=%fused_computation.19 | output fusion | flops 16777344 | bytes 17105408 | tf_op jit(solution)/shard_map/mul | solution.py:47
  95.7 9.0 %multiply_reduce_fusion.4 = (f32[32,4,128]{2,1,0:T(4,128)S(1)}, f32[32,4,128,128]{3,2,1,0:T(8,128)}) fusion(f32[32,4,128]{2,1,0:T(4,128)S(1)} %get-tuple-element.10, f32[32,4,128]{2,1,0:T(4,128)S(1)} %get-tuple-element.21, f32[32,4,128,128]{3,2,1,0:T(8,128)S(1)} %get-tuple-element.64, f32[32,4,128]{2,1,0:T(4,128)S(1)} %get-tuple-element.70, ...), kind=kOutput, calls=%fused_computation.15 | output fusion | flops 16777344 | bytes 17105408 | tf_op jit(solution)/shard_map/mul | solution.py:47
  104.7 14.0 %fusion = f32[32,4,128,128]{3,2,1,0:T(8,128)} fusion(f32[32,4,128]{2,1,0:T(4,128)S(1)} %get-tuple-element.72, f32[32,4,128,128]{3,2,1,0:T(8,128)} %get-tuple-element.62, f32[32,4,128]{2,1,0:T(4,128)S(1)} %get-tuple-element.20, f32[32,4,128]{2,1,0:T(4,128)S(1)} %get-tuple-element.12, f32[32,4]{1,0:T(8,128)S(1)} %bitcast.169, ...), kind=kOutput, calls=%fused_computation | output fusion | flops 14713086 | bytes 17039872 | tf_op jit(solution)/shard_map/mul | solution.py:47
  118.7 14.9 %multiply_reduce_fusion.2 = (f32[32,4,128]{2,1,0:T(4,128)S(1)}, f32[32,4,128]{2,1,0:T(4,128)S(1)}) fusion(f32[32,4,128]{2,1,0:T(4,128)} %get-tuple-element.9, f32[32,4,128]{2,1,0:T(4,128)S(1)} %get-tuple-element.19, f32[32,4,128,128]{3,2,1,0:T(8,128)} %fusion, f32[32,4,128]{2,1,0:T(4,128)S(1)} %get-tuple-element.11, f32[32,4]{1,0:T(8,128)S(1)} %bitcast.167, ...), kind=kOutput, calls=%fused_computation.11 | output fusion | flops 31441024 | bytes 17368064 | tf_op jit(solution)/shard_map/mul | solution.py:47
  133.6 0.3 multiply_reduce_fusion.13
  133.9 0.2 broadcast_multiply_fusion
  134.1 0.1 fusion.42
  134.2 0.2 broadcast_in_dim.4
  134.4 33.5 %all_to_all.29 = bf16[16,128,512]{2,1,0:T(8,128)(2,1)S(1)} all-to-all(bf16[16,128,512]{2,1,0:T(8,128)(2,1)S(1)} %broadcast_in_dim.4), channel_id=1, replica_groups=mesh['dp'=4,'kv'=16,'tp'=2] {'kv'}, dimensions={0} | all-to-all | bytes 4194304 | tf_op jit(solution)/shard_map/all_to_all | solution.py:15
  167.9 0.8 convolution_convert_fusion
  168.7 6.1 %all_to_all.30 = bf16[2,2048,64]{1,2,0:T(8,128)(2,1)S(1)} all-to-all(bf16[2,2048,64]{1,2,0:T(8,128)(2,1)S(1)} %bitcast.152), channel_id=1, replica_groups=mesh['dp'=4,'kv'=16,'tp'=2] {'tp'}, dimensions={0} | all-to-all | bytes 1048576 | tf_op jit(solution)/shard_map/all_to_all | solution.py:31
  175.0 0.1 broadcast_in_dim.5
  175.1 12.2 %all_to_all.31 = f32[32,1,2048]{2,1,0:T(1,128)S(1)} all-to-all(f32[32,1,2048]{2,1,0:T(1,128)S(1)} %broadcast_in_dim.5), channel_id=1, replica_groups=mesh['dp'=4,'kv'=16,'tp'=2] {'kv','tp'}, dimensions={0} | all-to-all | bytes 524288 | tf_op jit(solution)/shard_map/all_to_all | solution.py:15
  187.4 0.2 reduce_sum.199
  187.6 0.8 multiply_convert_fusion
  (46 shorter events, 1.1 us)
Async XLA Ops:
  0.6 74.6 %copy-start = (bf16[2048,512]{1,0:T(8,128)(2,1)S(1)}, bf16[2048,512]{1,0:T(8,128)(2,1)}, u32[]{:S(2)}) copy-start(bf16[2048,512]{1,0:T(8,128)(2,1)} %param.23) | copy-start | bytes 6291460
  0.6 64.0 %all-to-all-start = ((bf16[16,128,128]{2,1,0:T(8,128)(2,1)}), bf16[16,128,128]{2,1,0:T(8,128)(2,1)S(1)}, u32[]{:S(2)}, u32[]{:S(2)}) async-start(bf16[16,128,128]{2,1,0:T(8,128)(2,1)} %bitcast.154), calls=%async_computation | async-start | bytes 1048576 | tf_op jit(solution)/shard_map/all_to_all | solution.py:123
  57.5 11.0 %copy-start.8 = (f32[2048]{0:T(1024)S(1)}, f32[2048]{0:T(1024)}, u32[]{:S(2)}) copy-start(f32[2048]{0:T(1024)} %param.19) | copy-start | bytes 24580
  57.5 12.6 %copy-start.10 = (bf16[2048,8]{0,1:T(8,128)(2,1)S(1)}, bf16[2048,8]{0,1:T(8,128)(2,1)}, u32[]{:S(2)}) copy-start(bf16[2048,8]{0,1:T(8,128)(2,1)} %param.25) | copy-start | bytes 98308
  57.5 12.8 %copy-start.11 = (bf16[2048,8]{0,1:T(8,128)(2,1)S(1)}, bf16[2048,8]{0,1:T(8,128)(2,1)}, u32[]{:S(2)}) copy-start(bf16[2048,8]{0,1:T(8,128)(2,1)} %param.24) | copy-start | bytes 98308
  75.2 4.8 %copy-start.2 = (bf16[2048,512]{1,0:T(8,128)(2,1)S(1)}, bf16[2048,512]{1,0:T(8,128)(2,1)}, u32[]{:S(2)}) copy-start(bf16[2048,512]{1,0:T(8,128)(2,1)} %param.20) | copy-start | bytes 6291460
  77.9 5.3 %copy-start.7 = (f32[32,1,4]{2,0,1:T(8,128)S(1)}, f32[32,1,4]{2,0,1:T(8,128)}, u32[]{:S(2)}) copy-start(f32[32,1,4]{2,0,1:T(8,128)} %copy.113) | copy-start | bytes 1540
  83.2 21.5 %copy-start.4 = (f32[32,4,128]{2,1,0:T(4,128)}, f32[32,4,128]{2,1,0:T(4,128)S(1)}, u32[]{:S(2)}) copy-start(f32[32,4,128]{2,1,0:T(4,128)S(1)} %get-tuple-element.12) | copy-start | bytes 196612
  83.2 12.5 %copy-start.6 = (f32[32,1,4]{2,0,1:T(8,128)S(1)}, f32[32,1,4]{2,0,1:T(8,128)}, u32[]{:S(2)}) copy-start(f32[32,1,4]{2,0,1:T(8,128)} %copy.115) | copy-start | bytes 1540
  95.7 9.0 %copy-start.5 = (f32[32,1,4]{2,0,1:T(8,128)S(1)}, f32[32,1,4]{2,0,1:T(8,128)}, u32[]{:S(2)}) copy-start(f32[32,1,4]{2,0,1:T(8,128)} %copy.117) | copy-start | bytes 1540
  118.7 15.4 %copy-start.9 = (f32[512]{0:T(512)S(1)}, f32[512]{0:T(512)}, u32[]{:S(2)}) copy-start(f32[512]{0:T(512)} %broadcast_bitcast_fusion) | copy-start | bytes 6148
  118.7 49.2 %copy-start.3 = (bf16[512,128]{1,0:T(8,128)(2,1)S(1)}, bf16[512,128]{1,0:T(8,128)(2,1)}, u32[]{:S(2)}) copy-start(bf16[512,128]{1,0:T(8,128)(2,1)} %param.28) | copy-start | bytes 393220
  118.7 69.6 %copy-start.1 = (bf16[2048,512]{1,0:T(8,128)(2,1)S(1)}, bf16[2048,512]{1,0:T(8,128)(2,1)}, u32[]{:S(2)}) copy-start(bf16[2048,512]{1,0:T(8,128)(2,1)} %param.23) | copy-start | bytes 6291460
  133.6 54.0 %copy-start.12 = (f32[64]{0:T(128)S(1)}, f32[64]{0:T(128)}, u32[]{:S(2)}) copy-start(f32[64]{0:T(128)} %param.29) | copy-start | bytes 772
where the time goes:
time: 189 us; the launch traced here: 188 us
  other arithmetic  110 us (58%)
  blocking collectives  51.8 us (27%)
  local copies, waits for them, and re-layouts  10.8 us (6%)
  starting transfers between devices  8.73 us (5%)
  matrix products  6.39 us (3%)
    mul x10, other arithmetic, advance(): rate_cube * key_row[..., :, None] * recalled[..., None, :]  98.3 us
    all_to_all x2, blocking collectives, from_everyone(): lax.all_to_all(jnp.broadcast_to(shard[None], (count, *shard.shape)), axis...  45.7 us
    all_to_all x1, starting transfers between devices, local(): lax.all_to_all(tokens, 'kv', split_axis=0, concat_axis=1, tiled=True)  8.73 us
    all_to_all x1, blocking collectives, summed_on_arrival(): tiles = lax.all_to_all(cut_along(shard, dim, count), axis, 0, 0, tiled=True)  6.1 us
    dot_general x4, matrix products, local(): jnp.dot(scaled, weight, preferred_element_type=jnp.float32)  5.21 us
  transfers between devices with their start and end apart: 1, of which 0 were waited for; matrix products, arithmetic and copies ran while one was open for 29% of the time, Pallas kernels for 0%

commit v1 on v0

v1 whole, which is shorter than its diff:
```python
import functools
import jax
import jax.numpy as jnp
from jax import lax
from jax.experimental import pallas as pl
from jax.experimental.pallas import tpu as pltpu
from jax.sharding import PartitionSpec as P

F32 = jnp.float32
BF16 = jnp.bfloat16
EPS = 1e-06


def dot(a, b):
    return jnp.dot(a.astype(BF16), b.astype(BF16), preferred_element_type=F32)


def dot_t(a, b):
    return lax.dot_general(
        a.astype(BF16), b.astype(BF16), (((1,), (1,)), ((), ())), preferred_element_type=F32
    )


def unit(values):
    return values * lax.rsqrt(jnp.sum(values * values, axis=-1, keepdims=True) + EPS)


def silu(values):
    return values / (1.0 + jnp.exp(-values))


def chain_terms(log_decays, steps):
    rows = log_decays.shape[0]
    place = lax.broadcasted_iota(jnp.int32, log_decays.shape, 0) % steps
    total = log_decays
    shift = 1
    while shift < steps:
        total = total + jnp.where(place >= shift, pltpu.roll(total, shift, 0), 0.0)
        shift *= 2
    rest = jnp.where(place + 1 < steps, pltpu.roll(log_decays, rows - 1, 0), 0.0)
    shift = 1
    while shift < steps:
        rest = rest + jnp.where(place + shift < steps, pltpu.roll(rest, rows - shift, 0), 0.0)
        shift *= 2
    return total, rest


def chain_writes(keys, values, recalled, rates, total, steps):
    rows = keys.shape[0]
    row = lax.broadcasted_iota(jnp.int32, (rows, rows), 0)
    col = lax.broadcasted_iota(jnp.int32, (rows, rows), 1)
    same = row // steps == col // steps
    before = same & (col < row)
    gaps = total[:, :rows] - total[:, :rows].T
    fade = jnp.exp(jnp.where(same & (col <= row), gaps, 0.0))
    mix = jnp.where(before, rates * fade * dot_t(keys, keys), 0.0)
    start = rates * (values - jnp.exp(total[:, : values.shape[1]]) * recalled)
    done = start
    once = dot(mix, start)
    twice = dot(mix, once)
    done = start + twice
    done = done - dot(mix, done)
    return done, fade, same & (col <= row)


def by_sequence(left, states, steps):
    rows = left[0].shape[0]
    tile = 8
    per = tile // steps
    outs = [[] for _ in left]
    for first in range(0, rows, tile):
        stack = jnp.concatenate([part[first : first + tile] for part in left], axis=0)
        held = jnp.concatenate([states(first // steps + i) for i in range(per)], axis=1)
        size = held.shape[1] // per
        got = dot(stack, held)
        for index in range(len(left)):
            piece = got[index * tile : (index + 1) * tile]
            which = lax.broadcasted_iota(jnp.int32, (tile, size), 0) // steps
            value = piece[:, :size]
            for i in range(1, per):
                value = jnp.where(which == i, piece[:, i * size : (i + 1) * size], value)
            outs[index].append(value)
    return [jnp.concatenate(part, axis=0) for part in outs]


def commit_kernel(steps, state_ref, keys_ref, values_ref, coef_ref, out_ref):
    seqs, heads, size, _ = state_ref.shape
    span = seqs * steps
    rows = span * heads

    def stack(ref):
        return jnp.concatenate(
            [ref[:, h * size : (h + 1) * size].astype(F32) for h in range(heads)], axis=0
        )

    def column(first):
        return jnp.concatenate(
            [
                jnp.broadcast_to(coef_ref[:, first + h : first + h + 1], (span, size))
                for h in range(heads)
            ],
            axis=0,
        )

    keys = unit(stack(keys_ref))
    values = stack(values_ref)
    rates = column(0)
    total, rest = chain_terms(column(heads), steps)

    def state_of(index):
        return state_ref[index % seqs, index // seqs].astype(BF16)

    (recalled,) = by_sequence([keys], state_of, steps)
    writes, _, _ = chain_writes(keys, values, recalled, rates, total, steps)
    writes = jnp.exp(rest) * writes
    whole = jnp.exp(total + rest)
    keys_t = keys.T.astype(BF16)
    group = lax.broadcasted_iota(jnp.int32, (rows, size), 0) // steps
    for index in range(0, seqs * heads, 2):
        pair = jnp.concatenate(
            [jnp.where(group == index + i, writes, 0.0).astype(BF16) for i in range(2)], axis=1
        )
        added = jnp.dot(keys_t, pair, preferred_element_type=F32)
        for i in range(2):
            s, h = (index + i) % seqs, (index + i) // seqs
            scale = whole[(index + i) * steps : (index + i) * steps + 1]
            out_ref[s, h] = scale * state_ref[s, h] + added[:, i * size : (i + 1) * size]


def commit(saved_state, keys, values, coef, steps):
    seqs, heads, size, _ = saved_state.shape
    block = 8
    span = block * steps
    return pl.pallas_call(
        functools.partial(commit_kernel, steps),
        grid=(seqs // block,),
        out_shape=jax.ShapeDtypeStruct(saved_state.shape, F32),
        in_specs=[
            pl.BlockSpec((block, heads, size, size), lambda i: (i, 0, 0, 0)),
            pl.BlockSpec((span, heads * size), lambda i: (i, 0)),
            pl.BlockSpec((span, heads * size), lambda i: (i, 0)),
            pl.BlockSpec((span, coef.shape[1]), lambda i: (i, 0)),
        ],
        out_specs=pl.BlockSpec((block, heads, size, size), lambda i: (i, 0, 0, 0)),
        name="commit",
    )(saved_state, keys, values, coef)


def read_kernel(
    steps,
    tokens_ref,
    gain_ref,
    query_ref,
    key_ref,
    value_ref,
    gate_ref,
    small_ref,
    log_ref,
    head_gain_ref,
    state_ref,
    out_ref,
    scaled_ref,
    inverse_ref,
    coef_ref,
):
    head = pl.program_id(0)
    blocks, rows, width = tokens_ref.shape
    size = state_ref.shape[2]
    heads = log_ref.shape[1]

    @pl.when(head == 0)
    def _():
        squares = jnp.zeros((rows, width), F32)
        for j in range(blocks):
            wide = tokens_ref[j].astype(F32)
            squares = squares + wide * wide
            scaled_ref[:, j * width : (j + 1) * width] = (wide * gain_ref[j : j + 1]).astype(BF16)
        mean = jnp.sum(squares, axis=1, keepdims=True) / (blocks * width)
        inverse = lax.rsqrt(mean + EPS)
        inverse_ref[...] = jnp.broadcast_to(inverse, inverse_ref.shape)
        raw = jnp.dot(scaled_ref[...], small_ref[...], preferred_element_type=F32) * inverse
        rates = 1.0 / (1.0 + jnp.exp(-raw[:, :heads]))
        lift = raw[:, heads:]
        soft = jnp.maximum(lift, 0.0) + jnp.log1p(jnp.exp(-jnp.abs(lift)))
        coef_ref[:, :heads] = rates
        coef_ref[:, heads : 2 * heads] = -jnp.exp(log_ref[...]) * soft

    scaled = scaled_ref[...]
    inverse = inverse_ref[...]

    def project(ref):
        return jnp.dot(scaled, ref[...], preferred_element_type=F32) * inverse

    lane = lax.broadcasted_iota(jnp.int32, (rows, 2 * heads), 1)

    def column(index):
        picked = jnp.sum(jnp.where(lane == index, coef_ref[...], 0.0), axis=1, keepdims=True)
        return jnp.broadcast_to(picked, (rows, size))

    queries = unit(silu(project(query_ref))) * size ** (-0.5)
    keys = unit(silu(project(key_ref)))
    values = silu(project(value_ref))
    gates = silu(project(gate_ref))
    rates = column(head)
    total, _ = chain_terms(column(head + heads), steps)

    def state_of(index):
        return state_ref[index, 0].astype(BF16)

    recalled, seen = by_sequence([keys, queries], state_of, steps)
    writes, fade, upto = chain_writes(keys, values, recalled, rates, total, steps)
    weights = jnp.where(upto, fade * dot_t(queries, keys), 0.0)
    reads = jnp.exp(total) * seen + dot(weights, writes)
    mean = jnp.sum(reads * reads, axis=1, keepdims=True) / size
    out_ref[...] = (reads * lax.rsqrt(mean + EPS) * head_gain_ref[...] * gates).astype(BF16)


def read(tokens, gain, weights, small, decay_log, head_gain, committed, steps):
    blocks, rows, width = tokens.shape
    seqs, heads, size, _ = committed.shape
    model = blocks * width
    whole = lambda *shape: pl.BlockSpec(shape, lambda i: (0,) * len(shape))
    return pl.pallas_call(
        functools.partial(read_kernel, steps),
        grid=(heads,),
        out_shape=jax.ShapeDtypeStruct((rows, heads * size), BF16),
        in_specs=[
            whole(blocks, rows, width),
            whole(blocks, width),
            *[pl.BlockSpec((model, size), lambda i: (0, i)) for _ in range(4)],
            whole(model, 2 * heads),
            whole(1, heads),
            whole(1, size),
            pl.BlockSpec((seqs, 1, size, size), lambda i: (0, i, 0, 0)),
        ],
        out_specs=pl.BlockSpec((rows, size), lambda i: (0, i)),
        scratch_shapes=[
            pltpu.VMEM((rows, model), BF16),
            pltpu.VMEM((rows, size), F32),
            pltpu.VMEM((rows, 2 * heads), F32),
        ],
        name="read",
    )(tokens, gain, *weights, small, decay_log, head_gain, committed)


def project_kernel(left_ref, right_ref, weight_ref, out_ref, square_ref):
    blocks, depth, width = weight_ref.shape
    half = width // 2
    rows = left_ref.shape[0]
    left = left_ref[...]
    right = right_ref[...]
    squares = jnp.zeros((rows, half), F32)
    for j in range(blocks):
        both = weight_ref[j]
        first = jnp.dot(left, both, preferred_element_type=F32)
        second = jnp.dot(right, both, preferred_element_type=F32)
        value = first[:, :half] + second[:, half:]
        squares = squares + value * value
        out_ref[j] = value
    total = jnp.sum(squares, axis=1, keepdims=True)
    square_ref[...] = jnp.broadcast_to(total, square_ref.shape)


def project(left, right, weight):
    blocks, depth, width = weight.shape
    rows = left.shape[0]
    return pl.pallas_call(
        project_kernel,
        out_shape=(
            jax.ShapeDtypeStruct((blocks, rows, width // 2), F32),
            jax.ShapeDtypeStruct((rows, 128), F32),
        ),
        name="project",
    )(left, right, weight)


def normalize_kernel(model, value_ref, mine_ref, other_ref, out_ref):
    blocks, rows, half = value_ref.shape
    total = mine_ref[:, :half] + other_ref[:, :half]
    factor = lax.rsqrt(total / model + EPS)
    for j in range(blocks):
        value = value_ref[j] * factor
        out_ref[j] = jnp.concatenate([value[: rows // 2], value[rows // 2 :]], axis=1).astype(BF16)


def normalize(value, mine, other, model):
    blocks, rows, half = value.shape
    return pl.pallas_call(
        functools.partial(normalize_kernel, model),
        out_shape=jax.ShapeDtypeStruct((blocks, rows // 2, 2 * half), BF16),
        name="normalize",
    )(value, mine, other)


def spread_kernel(value_ref, gain_ref, out_ref):
    blocks, rows, width = value_ref.shape
    half = width // 2
    gain = gain_ref[...]
    for j in range(blocks):
        value = value_ref[j].astype(F32)
        base = 2 * rows * j
        out_ref[base : base + rows] = (value[:, :half] * gain).astype(BF16)
        out_ref[base + rows : base + 2 * rows] = (value[:, half:] * gain).astype(BF16)


def spread(value, gain):
    blocks, rows, width = value.shape
    return pl.pallas_call(
        spread_kernel,
        out_shape=jax.ShapeDtypeStruct((blocks * rows * 2, width // 2), BF16),
        name="spread",
    )(value, gain)


def local(
    tokens,
    pre_gain,
    query_weight,
    key_weight,
    value_weight,
    gate_weight,
    beta_weight,
    decay_weight,
    decay_log,
    head_gain,
    out_weight,
    post_gain,
    saved_state,
    earlier_keys,
    earlier_values,
    earlier_rates,
    earlier_decays,
    accepted,
):
    seqs, heads, size, _ = saved_state.shape
    steps = earlier_keys.shape[1]
    rows = seqs * steps
    model = pre_gain.shape[0]
    groups = lax.axis_size("kv")
    core = lax.axis_index("tp")
    swap = [(0, 1), (1, 0)]

    own = lax.all_to_all(
        tokens.reshape(groups, rows, tokens.shape[1]), "kv", 0, 0, tiled=True
    )
    depth, cols = out_weight.shape
    half = cols // 2
    keep = lax.dynamic_slice_in_dim(out_weight, core * half, half, 1)
    give = lax.dynamic_slice_in_dim(out_weight, (1 - core) * half, half, 1)
    got = lax.ppermute(give, "tp", swap)
    both = jnp.concatenate([keep, got], axis=1)
    wide = lax.all_to_all(
        jnp.broadcast_to(both[None], (groups, depth, cols)), "kv", 0, 0, tiled=True
    )

    live = jnp.arange(steps)[None, :, None] < accepted[:, None, None]
    coef = jnp.concatenate(
        [jnp.where(live, earlier_rates, 0.0), jnp.where(live, earlier_decays, 0.0)], axis=2
    ).reshape(rows, 2 * heads)
    committed = commit(
        saved_state,
        earlier_keys.reshape(rows, heads * size),
        earlier_values.reshape(rows, heads * size),
        coef,
        steps,
    )
    small = jnp.concatenate(
        [
            lax.dynamic_slice_in_dim(weight, core * heads, heads, 1)
            for weight in (beta_weight, decay_weight)
        ],
        axis=1,
    )
    attended = read(
        own,
        pre_gain.reshape(groups, -1),
        (query_weight, key_weight, value_weight, gate_weight),
        small,
        decay_log.reshape(1, heads),
        head_gain.reshape(1, size),
        committed,
        steps,
    )
    other = lax.ppermute(attended, "tp", swap)
    value, mine = project(attended, other, wide)
    theirs = lax.ppermute(mine, "tp", swap)
    packed = normalize(value, mine, theirs, model)
    arrived = lax.all_to_all(packed, "kv", 0, 0, tiled=True)
    mixed = spread(arrived, post_gain.reshape(1, half))
    return (mixed, committed)


def solution(mesh):
    placed = (
        P("dp", "kv"),
        P(),
        P(None, "tp"),
        P(None, "tp"),
        P(None, "tp"),
        P(None, "tp"),
        P(),
        P(),
        P("tp"),
        P(),
        P("tp", "kv"),
        P(("kv", "tp")),
        P(("dp", "kv"), "tp", None, None),
        P(("dp", "kv"), None, "tp", None),
        P(("dp", "kv"), None, "tp", None),
        P(("dp", "kv"), None, "tp"),
        P(("dp", "kv"), None, "tp"),
        P(("dp", "kv")),
    )
    return jax.shard_map(
        local,
        mesh=mesh,
        in_specs=placed,
        out_specs=(P("dp", ("kv", "tp")), P(("dp", "kv"), "tp", None, None)),
        check_vma=False,
    )
```

time: 189 us -> 83.3 us (0.44)
  other arithmetic: 110 us -> 0.16 us
  blocking collectives: 51.8 us -> 12.6 us
  Pallas kernels: 0 us -> 28.4 us
  waiting for transfers between devices: 0.01 us -> 11.7 us
  starting transfers between devices: 8.73 us -> 19.9 us
  matrix products: 6.39 us -> 0 us
    mul x19 -> x0, other arithmetic: 101 us -> none  [the longest x10 98.3 us: advance(): rate_cube * key_row[..., :, None] * recalled[..., None, :]]
    all_to_all x3 -> x1, blocking collectives: 51.8 us -> 12.6 us  [local(): arrived = lax.all_to_all(packed, 'kv', 0, 0, tiled=True)]
    pallas_call x0 -> x5, Pallas kernels: none -> 28.4 us  [the longest x1 10.8 us: read(): pl.pallas_call(functools.partial(read_kernel, steps), grid=(heads,), out_...]
    all_to_all x1 -> x2, waiting for transfers between devices: 0.01 us -> 8.36 us  [the longest x1 7.16 us: local(): lax.all_to_all(tokens.reshape(groups, rows, tokens.shape[1]), 'kv', 0, 0,...]
    ppermute x0 -> x3, starting transfers between devices: none -> 7.45 us  [the longest x1 4.35 us: local(): theirs = lax.ppermute(mine, 'tp', swap)]
    dot_general x7 -> x0, matrix products: 6.39 us -> none  [the longest x4 5.21 us: local(): jnp.dot(scaled, weight, preferred_element_type=jnp.float32)]
    convert_element_type x6 -> x0, other arithmetic: 5.13 us -> none  [the longest x1 1.56 us: local(): scaled = (widened * pre_gain).astype(jnp.bfloat16)]
    unnamed x26 -> x23, local copies, waits for them, and re-layouts: 0.07 us -> 3.92 us
  transfers between devices with their start and end apart: 1 -> 5, of which waited for: 0 -> 5; matrix products, arithmetic and copies ran while one was open for 29% -> 5% of each run, Pallas kernels for 0% -> 24%
where the time goes in v1:
time: 83.3 us; the launch traced here: 82.7 us
  Pallas kernels  28.4 us (34%)
  starting transfers between devices  19.9 us (24%)
  blocking collectives  12.6 us (15%)
  waiting for transfers between devices  11.7 us (14%)
  local copies, waits for them, and re-layouts  9.24 us (11%)
    all_to_all x1, blocking collectives, local(): arrived = lax.all_to_all(packed, 'kv', 0, 0, tiled=True)  12.6 us
    pallas_call x1, Pallas kernels, read(): pl.pallas_call(functools.partial(read_kernel, steps), grid=(heads,), out_...  10.8 us
    pallas_call x1, Pallas kernels, commit(): pl.pallas_call(functools.partial(commit_kernel, steps), grid=(seqs // blo...  9.38 us
    all_to_all x1, starting transfers between devices, local(): lax.all_to_all(tokens.reshape(groups, rows, tokens.shape[1]), 'kv', 0, 0,...  8.6 us
    all_to_all x1, waiting for transfers between devices, local(): lax.all_to_all(tokens.reshape(groups, rows, tokens.shape[1]), 'kv', 0, 0,...  7.16 us
    ppermute x1, starting transfers between devices, local(): theirs = lax.ppermute(mine, 'tp', swap)  4.35 us
    pallas_call x1, Pallas kernels, project(): pl.pallas_call(project_kernel, out_shape=(jax.ShapeDtypeStruct((blocks, r...  4.08 us
    unnamed x23, local copies, waits for them, and re-layouts  3.92 us
  transfers between devices with their start and end apart: 5, of which 5 were waited for; matrix products, arithmetic and copies ran while one was open for 5% of the time, Pallas kernels for 24%

profile of v1, /device:TPU:1, one launch (start us, length us, event | category | flops | bytes accessed | tf_op | source)
XLA Modules:
  0.0 82.7 jit_solution(17216612527131014967)
XLA Ops:
  0.6 8.6 %all-to-all-start = ((bf16[16,128,128]{2,1,0:T(8,128)(2,1)}), bf16[16,128,128]{2,1,0:T(8,128)(2,1)S(1)}, u32[]{:S(2)}, u32[]{:S(2)}) async-start(bf16[16,128,128]{2,1,0:T(8,128)(2,1)} %bitcast.14), calls=%async_computation | async-start | bytes 1048576 | tf_op jit(solution)/shard_map/all_to_all | solution.py:343
  9.2 1.1 %constant_dynamic-slice_fusion.1 = (bf16[512,64]{1,0:T(8,128)(2,1)S(1)}, bf16[512,64]{1,0:T(8,128)(2,1)S(1)}) fusion(bf16[512,128]{1,0:T(8,128)(2,1)} %param.28, s32[]{:T(128)S(6)} %select_n.20, s32[]{:T(128)S(6)} %select_n.21), kind=kLoop, calls=%fused_computation.9 | loop fusion | bytes 262152 | tf_op jit(solution)/shard_map/dynamic_slice | solution.py:348
  10.4 1.0 %collective-permute-start.1 = (bf16[512,64]{1,0:T(8,128)(2,1)S(1)}, bf16[512,64]{1,0:T(8,128)(2,1)S(1)}, u32[]{:S(2)}, u32[]{:S(2)}) collective-permute-start(bf16[512,64]{1,0:T(8,128)(2,1)S(1)} %get-tuple-element.11), channel_id=1, source_target_pairs={{0,1},{1,0},{2,3},{3,2},{4,5},{5,4},{6,7},{7,6},{8,9},{9,8},{10,11... | collective-permute-start | bytes 196616 | tf_op jit(solution)/shard_map/ppermute | solution.py:350
  11.4 1.0 %collective-permute-done.1 = bf16[512,64]{1,0:T(8,128)(2,1)S(1)} collective-permute-done((bf16[512,64]{1,0:T(8,128)(2,1)S(1)}, bf16[512,64]{1,0:T(8,128)(2,1)S(1)}, u32[]{:S(2)}, u32[]{:S(2)}) %collective-permute-start.1) | collective-permute-done | bytes 65568 | tf_op jit(solution)/shard_map/ppermute | solution.py:350
  12.4 0.1 pad_maximum_fusion
  12.5 7.2 %all-to-all-done.tokens_ref = bf16[16,128,128]{2,1,0:T(8,128)(2,1)S(1)} async-done(((bf16[16,128,128]{2,1,0:T(8,128)(2,1)}), bf16[16,128,128]{2,1,0:T(8,128)(2,1)S(1)}, u32[]{:S(2)}, u32[]{:S(2)}) %all-to-all-start) | async-done | bytes 524320 | tf_op jit(solution)/shard_map/all_to_all | solution.py:343
  19.7 0.0 copy-start.1
  19.7 1.7 %broadcast_in_dim.26 = bf16[16,512,128]{2,1,0:T(8,128)(2,1)} broadcast(bf16[512,128]{1,0:T(8,128)(2,1)S(1)} %pad_maximum_fusion), dimensions={1,2} | broadcast | bytes 2228224 | tf_op jit(solution)/shard_map/broadcast_in_dim | solution.py:353
  21.4 0.0 copy-start.10
  21.4 0.0 copy-start.8
  21.4 0.0 copy-start.9
  21.4 0.0 copy-start.6
  21.4 0.0 copy-start.7
  21.4 0.0 copy-start.3
  21.4 0.0 copy-start.4
  21.4 0.0 copy-done.1
  21.5 3.9 %all-to-all-start.1 = ((bf16[16,512,128]{2,1,0:T(8,128)(2,1)}), bf16[16,512,128]{2,1,0:T(8,128)(2,1)S(1)}, u32[]{:S(2)}, u32[]{:S(2)}) async-start(bf16[16,512,128]{2,1,0:T(8,128)(2,1)} %broadcast_in_dim.26), calls=%async_computation.1 | async-start | bytes 4194304 | tf_op jit(solution)/shard_map/all_to_all | solution.py:352
  25.3 0.0 copy-done.10
  25.3 0.0 copy-done.8
  25.4 0.0 copy-done.9
  25.4 0.7 copy.24
  26.1 0.0 copy-done.6
  26.1 0.0 copy-done.7
  26.2 1.0 %copy.25.small_ref = bf16[2048,8]{1,0:T(8,128)(2,1)} copy(bf16[2048,8]{0,1:T(8,128)(2,1)S(1)} %pad_maximum_fusion.1) | data formatting | bytes 65536 | tf_op jit(solution)/shard_map/concatenate | solution.py:367
  27.2 0.0 copy-done.3
  27.2 0.0 copy-done.4
  27.2 0.7 copy_bitcast_fusion
  27.9 9.4 %commit.1.state_ref = f32[32,4,128,128]{3,2,1,0:T(8,128)} custom-call(f32[32,4,128,128]{3,2,1,0:T(8,128)} %state_ref.1, bf16[128,512]{1,0:T(8,128)(2,1)} %get-tuple-element.17.keys_ref, bf16[128,512]{1,0:T(8,128)(2,1)} %get-tuple-element.16.values_ref, f32[128,8]{1,0:T(8,128)} %bitcast.15), custom_call_target="tpu_custom_call" | custom-call | tf_op jit(solution)/shard_map/commit/pallas_call | solution.py:134
  37.3 10.8 %read.1.left_ref = bf16[128,512]{1,0:T(8,128)(2,1)} custom-call(bf16[16,128,128]{2,1,0:T(8,128)(2,1)} %copy-done.1, f32[16,128]{1,0:T(8,128)} %bitcast.18, bf16[2048,512]{1,0:T(8,128)(2,1)} %query_ref.1, bf16[2048,512]{1,0:T(8,128)(2,1)} %key_ref.1, bf16[2048,512]{1,0:T(8,128)(2,1)} %value_ref.1, bf16[2048,512]{1,0:T(8,128)(2,1)} %gate_ref.1, ...), custom_call_target="tpu_custom_call" | custom-call | tf_op jit(solution)/shard_map/read/pallas_call | solution.py:223
  48.0 2.1 %collective-permute-start = (bf16[128,512]{1,0:T(8,128)(2,1)}, bf16[128,512]{1,0:T(8,128)(2,1)S(1)}, u32[]{:S(2)}, u32[]{:S(2)}) collective-permute-start(bf16[128,512]{1,0:T(8,128)(2,1)} %read.1.left_ref), channel_id=1, source_target_pairs={{0,1},{1,0},{2,3},{3,2},{4,5},{5,4},{6,7},{7,6},{8,9},{9,8},{10,11... | collective-permute-start | bytes 393224 | tf_op jit(solution)/shard_map/ppermute | solution.py:384
  50.1 1.2 %collective-permute-done.right_ref = bf16[128,512]{1,0:T(8,128)(2,1)S(1)} collective-permute-done((bf16[128,512]{1,0:T(8,128)(2,1)}, bf16[128,512]{1,0:T(8,128)(2,1)S(1)}, u32[]{:S(2)}, u32[]{:S(2)}) %collective-permute-start) | collective-permute-done | bytes 131104 | tf_op jit(solution)/shard_map/ppermute | solution.py:384
  51.3 0.0 copy-start.2
  51.3 1.2 %all-to-all-done.1.weight_ref = bf16[16,512,128]{2,1,0:T(8,128)(2,1)S(1)} async-done(((bf16[16,512,128]{2,1,0:T(8,128)(2,1)}), bf16[16,512,128]{2,1,0:T(8,128)(2,1)S(1)}, u32[]{:S(2)}, u32[]{:S(2)}) %all-to-all-start.1) | async-done | bytes 2097184 | tf_op jit(solution)/shard_map/all_to_all | solution.py:352
  52.5 0.0 copy-done.2
  52.5 0.0 copy-start
  52.5 1.3 %copy-done = bf16[16,512,128]{2,1,0:T(8,128)(2,1)} copy-done((bf16[16,512,128]{2,1,0:T(8,128)(2,1)}, bf16[16,512,128]{2,1,0:T(8,128)(2,1)S(1)}, u32[]{:S(2)}) %copy-start) | copy-done | bytes 2097176
  53.9 4.1 %project.1 = (f32[16,128,64]{2,1,0:T(8,128)}, f32[128,128]{1,0:T(8,128)}) custom-call(bf16[128,512]{1,0:T(8,128)(2,1)} %read.1.left_ref, bf16[128,512]{1,0:T(8,128)(2,1)} %copy-done.2, bf16[16,512,128]{2,1,0:T(8,128)(2,1)} %copy-done), custom_call_target="tpu_custom_call" | custom-call | tf_op jit(solution)/shard_map/project/pallas_call | solution.py:267
  57.9 4.3 %collective-permute-start.2 = (f32[128,128]{1,0:T(8,128)}, f32[128,128]{1,0:T(8,128)S(1)}, u32[]{:S(2)}, u32[]{:S(2)}) collective-permute-start(f32[128,128]{1,0:T(8,128)} %get-tuple-element.5.mine_ref), channel_id=1, source_target_pairs={{0,1},{1,0},{2,3},{3,2},{4,5},{5,4},{6,7},{7,6},{8,9},{9,8},{10,11... | collective-permute-start | bytes 196616 | tf_op jit(solution)/shard_map/ppermute | solution.py:386
  62.3 1.1 %collective-permute-done.2.other_ref = f32[128,128]{1,0:T(8,128)S(1)} collective-permute-done((f32[128,128]{1,0:T(8,128)}, f32[128,128]{1,0:T(8,128)S(1)}, u32[]{:S(2)}, u32[]{:S(2)}) %collective-permute-start.2) | collective-permute-done | bytes 65568 | tf_op jit(solution)/shard_map/ppermute | solution.py:386
  63.4 0.0 copy-start.5
  63.4 0.6 copy-done.5
  64.0 2.1 %normalize.1 = bf16[16,64,128]{2,1,0:T(8,128)(2,1)} custom-call(f32[16,128,64]{2,1,0:T(8,128)} %get-tuple-element.4.value_ref, f32[128,128]{1,0:T(8,128)} %get-tuple-element.5.mine_ref, f32[128,128]{1,0:T(8,128)} %copy-done.5), custom_call_target="tpu_custom_call" | custom-call | tf_op jit(solution)/shard_map/normalize/pallas_call | solution.py:288
  66.1 12.6 %all_to_all.15.value_ref = bf16[16,64,128]{2,1,0:T(8,128)(2,1)} all-to-all(bf16[16,64,128]{2,1,0:T(8,128)(2,1)} %normalize.1), channel_id=1, replica_groups=mesh['dp'=4,'kv'=16,'tp'=2] {'kv'}, dimensions={0} | all-to-all | bytes 524288 | tf_op jit(solution)/shard_map/all_to_all | solution.py:388
  78.7 2.0 %spread.1 = bf16[2048,64]{1,0:T(8,128)(2,1)} custom-call(bf16[16,64,128]{2,1,0:T(8,128)(2,1)} %all_to_all.15.value_ref, f32[1,64]{1,0:T(1,128)} %bitcast.21), custom_call_target="tpu_custom_call" | custom-call | tf_op jit(solution)/shard_map/spread/pallas_call | solution.py:308
  80.8 1.9 %copy.26 = bf16[2048,64]{0,1:T(8,128)(2,1)} copy(bf16[2048,64]{1,0:T(8,128)(2,1)} %spread.1) | data formatting | bytes 524288
  (5 shorter events, 0.1 us)
Async XLA Ops:
  0.6 19.0 %all-to-all-start = ((bf16[16,128,128]{2,1,0:T(8,128)(2,1)}), bf16[16,128,128]{2,1,0:T(8,128)(2,1)S(1)}, u32[]{:S(2)}, u32[]{:S(2)}) async-start(bf16[16,128,128]{2,1,0:T(8,128)(2,1)} %bitcast.14), calls=%async_computation | async-start | bytes 1048576 | tf_op jit(solution)/shard_map/all_to_all | solution.py:343
  10.4 2.0 %collective-permute-start.1 = (bf16[512,64]{1,0:T(8,128)(2,1)S(1)}, bf16[512,64]{1,0:T(8,128)(2,1)S(1)}, u32[]{:S(2)}, u32[]{:S(2)}) collective-permute-start(bf16[512,64]{1,0:T(8,128)(2,1)S(1)} %get-tuple-element.11), channel_id=1, source_target_pairs={{0,1},{1,0},{2,3},{3,2},{4,5},{5,4},{6,7},{7,6},{8,9},{9,8},{10,11... | collective-permute-start | bytes 196616 | tf_op jit(solution)/shard_map/ppermute | solution.py:350
  19.7 1.8 %copy-start.1 = (bf16[16,128,128]{2,1,0:T(8,128)(2,1)}, bf16[16,128,128]{2,1,0:T(8,128)(2,1)S(1)}, u32[]{:S(2)}) copy-start(bf16[16,128,128]{2,1,0:T(8,128)(2,1)S(1)} %all-to-all-done.tokens_ref) | copy-start | bytes 1572868
  21.4 3.9 %copy-start.10 = (s32[32]{0:T(128)S(1)}, s32[32]{0:T(128)}, u32[]{:S(2)}) copy-start(s32[32]{0:T(128)} %param.35) | copy-start | bytes 388
  21.4 3.9 %copy-start.8 = (f32[32,4,4]{0,2,1:T(4,128)S(1)}, f32[32,4,4]{0,2,1:T(4,128)}, u32[]{:S(2)}) copy-start(f32[32,4,4]{0,2,1:T(4,128)} %param.33) | copy-start | bytes 6148
  21.4 4.0 %copy-start.9 = (f32[32,4,4]{0,2,1:T(4,128)S(1)}, f32[32,4,4]{0,2,1:T(4,128)}, u32[]{:S(2)}) copy-start(f32[32,4,4]{0,2,1:T(4,128)} %param.34) | copy-start | bytes 6148
  21.4 4.7 %copy-start.6 = (bf16[2048,8]{0,1:T(8,128)(2,1)S(1)}, bf16[2048,8]{0,1:T(8,128)(2,1)}, u32[]{:S(2)}) copy-start(bf16[2048,8]{0,1:T(8,128)(2,1)} %param.25) | copy-start | bytes 98308
  21.4 4.7 %copy-start.7 = (bf16[2048,8]{0,1:T(8,128)(2,1)S(1)}, bf16[2048,8]{0,1:T(8,128)(2,1)}, u32[]{:S(2)}) copy-start(bf16[2048,8]{0,1:T(8,128)(2,1)} %param.24) | copy-start | bytes 98308
  21.4 5.8 %copy-start.3 = (bf16[32,4,4,128]{3,2,1,0:T(4,128)(2,1)S(1)}, bf16[32,4,4,128]{3,2,1,0:T(4,128)(2,1)}, u32[]{:S(2)}) copy-start(bf16[32,4,4,128]{3,2,1,0:T(4,128)(2,1)} %param.32) | copy-start | bytes 393220
  21.4 5.8 %copy-start.4 = (bf16[32,4,4,128]{3,2,1,0:T(4,128)(2,1)S(1)}, bf16[32,4,4,128]{3,2,1,0:T(4,128)(2,1)}, u32[]{:S(2)}) copy-start(bf16[32,4,4,128]{3,2,1,0:T(4,128)(2,1)} %param.31) | copy-start | bytes 393220
  21.5 31.1 %all-to-all-start.1 = ((bf16[16,512,128]{2,1,0:T(8,128)(2,1)}), bf16[16,512,128]{2,1,0:T(8,128)(2,1)S(1)}, u32[]{:S(2)}, u32[]{:S(2)}) async-start(bf16[16,512,128]{2,1,0:T(8,128)(2,1)} %broadcast_in_dim.26), calls=%async_computation.1 | async-start | bytes 4194304 | tf_op jit(solution)/shard_map/all_to_all | solution.py:352
  48.0 3.3 %collective-permute-start = (bf16[128,512]{1,0:T(8,128)(2,1)}, bf16[128,512]{1,0:T(8,128)(2,1)S(1)}, u32[]{:S(2)}, u32[]{:S(2)}) collective-permute-start(bf16[128,512]{1,0:T(8,128)(2,1)} %read.1.left_ref), channel_id=1, source_target_pairs={{0,1},{1,0},{2,3},{3,2},{4,5},{5,4},{6,7},{7,6},{8,9},{9,8},{10,11... | collective-permute-start | bytes 393224 | tf_op jit(solution)/shard_map/ppermute | solution.py:384
  51.3 1.2 %copy-start.2 = (bf16[128,512]{1,0:T(8,128)(2,1)}, bf16[128,512]{1,0:T(8,128)(2,1)S(1)}, u32[]{:S(2)}) copy-start(bf16[128,512]{1,0:T(8,128)(2,1)S(1)} %collective-permute-done.right_ref) | copy-start | bytes 393220
  52.5 1.3 %copy-start = (bf16[16,512,128]{2,1,0:T(8,128)(2,1)}, bf16[16,512,128]{2,1,0:T(8,128)(2,1)S(1)}, u32[]{:S(2)}) copy-start(bf16[16,512,128]{2,1,0:T(8,128)(2,1)S(1)} %all-to-all-done.1.weight_ref) | copy-start | bytes 6291460
  57.9 5.5 %collective-permute-start.2 = (f32[128,128]{1,0:T(8,128)}, f32[128,128]{1,0:T(8,128)S(1)}, u32[]{:S(2)}, u32[]{:S(2)}) collective-permute-start(f32[128,128]{1,0:T(8,128)} %get-tuple-element.5.mine_ref), channel_id=1, source_target_pairs={{0,1},{1,0},{2,3},{3,2},{4,5},{5,4},{6,7},{7,6},{8,9},{9,8},{10,11... | collective-permute-start | bytes 196616 | tf_op jit(solution)/shard_map/ppermute | solution.py:386
  63.4 0.6 copy-start.5

commit v2 on v1

v2 whole, which is shorter than its diff:
```python
import functools
import jax
import jax.numpy as jnp
from jax import lax
from jax.experimental import pallas as pl
from jax.experimental.pallas import tpu as pltpu
from jax.sharding import PartitionSpec as P

F32 = jnp.float32
BF16 = jnp.bfloat16
EPS = 1e-06
AHEAD = 4
READ_AHEAD = 6
CUTS = 2
Y = 4
TEAM = 2
VMEM = pltpu.VMEM
WHOLE = pl.BlockSpec(memory_space=pltpu.VMEM)
FAR = pl.BlockSpec(memory_space=pltpu.HBM)
SCALAR = pl.BlockSpec(memory_space=pltpu.SMEM)


def params(mib):
    return pltpu.CompilerParams(vmem_limit_bytes=mib * 1024 * 1024)


def near(value):
    return pltpu.with_memory_space_constraint(value, pltpu.VMEM)


def far(value):
    return pltpu.with_memory_space_constraint(value, pltpu.HBM)


def dot(a, b):
    return jnp.dot(a.astype(BF16), b.astype(BF16), preferred_element_type=F32)


def dot_t(a, b):
    return lax.dot_general(
        a.astype(BF16), b.astype(BF16), (((1,), (1,)), ((), ())), preferred_element_type=F32
    )


def unit(values):
    return values * lax.rsqrt(jnp.sum(values * values, axis=-1, keepdims=True) + EPS)


def silu(values):
    return values / (1.0 + jnp.exp(-values))


def chain_terms(log_decays, steps):
    rows = log_decays.shape[0]
    place = lax.broadcasted_iota(jnp.int32, log_decays.shape, 0) % steps
    total = log_decays
    shift = 1
    while shift < steps:
        total = total + jnp.where(place >= shift, pltpu.roll(total, shift, 0), 0.0)
        shift *= 2
    rest = jnp.where(place + 1 < steps, pltpu.roll(log_decays, rows - 1, 0), 0.0)
    shift = 1
    while shift < steps:
        rest = rest + jnp.where(place + shift < steps, pltpu.roll(rest, rows - shift, 0), 0.0)
        shift *= 2
    return total, rest


def chain_mix(keys, rates, total, steps):
    rows = keys.shape[0]
    row = lax.broadcasted_iota(jnp.int32, (rows, rows), 0)
    col = lax.broadcasted_iota(jnp.int32, (rows, rows), 1)
    upto = (row // steps == col // steps) & (col <= row)
    fade = jnp.exp(jnp.where(upto, total - total.T, 0.0))
    mix = jnp.where(upto & (col < row), rates * fade * dot_t(keys, keys), 0.0)
    return mix.astype(BF16), jnp.where(upto, fade, 0.0)


def chain_writes(mix, start):
    done = start + dot(mix, dot(mix, start))
    return done - dot(mix, done)


def by_sequence(left, states, steps):
    rows = left[0].shape[0]
    tile = 8
    per = tile // steps
    outs = [[] for _ in left]
    for first in range(0, rows, tile):
        stack = jnp.concatenate([part[first : first + tile] for part in left], axis=0)
        held = jnp.concatenate([states(first // steps + i) for i in range(per)], axis=1)
        size = held.shape[1] // per
        got = dot(stack, held)
        which = lax.broadcasted_iota(jnp.int32, (tile, size), 0) // steps
        for index in range(len(left)):
            piece = got[index * tile : (index + 1) * tile]
            value = piece[:, :size]
            for i in range(1, per):
                value = jnp.where(which == i, piece[:, i * size : (i + 1) * size], value)
            outs[index].append(value)
    return [jnp.concatenate(part, axis=0) for part in outs]


def recall_kernel(
    steps,
    source_ref,
    keys_ref,
    values_ref,
    coef_ref,
    state_ref,
    unit_ref,
    writes_ref,
    whole_ref,
    held_ref,
    short_ref,
    in_sems,
    out_sems,
):
    heads, seqs, size, _ = held_ref.shape
    rows = seqs * steps
    arrive = [
        pltpu.make_async_copy(source_ref.at[:, h], held_ref.at[h], in_sems.at[h])
        for h in range(heads)
    ]
    leave = [
        pltpu.make_async_copy(short_ref.at[h], state_ref.at[h], out_sems.at[h])
        for h in range(heads)
    ]
    for copy in arrive[:AHEAD]:
        copy.start()
    ready = []
    for h in range(heads):
        lanes = slice(h * size, (h + 1) * size)
        keys = unit(keys_ref[:, lanes].astype(F32))
        rates = jnp.broadcast_to(coef_ref[:, h : h + 1], (rows, size))
        total, rest = chain_terms(
            jnp.broadcast_to(coef_ref[:, heads + h : heads + h + 1], (rows, size)), steps
        )
        mix, _ = chain_mix(keys, rates, total, steps)
        unit_ref[:, lanes] = keys.astype(BF16)
        whole_ref[:, lanes] = jnp.exp(total + rest)
        given = rates * values_ref[:, lanes].astype(F32)
        ready.append((keys, mix, given, rates * jnp.exp(total), jnp.exp(rest)))
    starts = []
    for h in range(heads):
        keys, mix, given, scale, _ = ready[h]
        arrive[h].wait()
        if h + AHEAD < heads:
            arrive[h + AHEAD].start()
        short_ref[h] = held_ref[h].astype(BF16)
        leave[h].start()
        (recalled,) = by_sequence([keys], lambda s: short_ref[h, s], steps)
        starts.append(given - scale * recalled)
    for h in range(heads):
        lanes = slice(h * size, (h + 1) * size)
        writes_ref[:, lanes] = (ready[h][4] * chain_writes(ready[h][1], starts[h])).astype(BF16)
    for copy in leave:
        copy.wait()


def recall(state, keys, values, coef, steps):
    rows, width = keys.shape
    seqs, heads, size, _ = state.shape
    turned = (heads, seqs, size, size)
    return pl.pallas_call(
        functools.partial(recall_kernel, steps),
        out_shape=(
            pltpu.HBM(turned, BF16),
            VMEM((rows, width), BF16),
            VMEM((rows, width), BF16),
            VMEM((rows, width), F32),
        ),
        in_specs=[FAR] + [WHOLE] * 3,
        out_specs=(FAR,) + (WHOLE,) * 3,
        scratch_shapes=[
            pltpu.VMEM(turned, F32),
            pltpu.VMEM(turned, BF16),
            pltpu.SemaphoreType.DMA((heads,)),
            pltpu.SemaphoreType.DMA((heads,)),
        ],
        compiler_params=params(20),
        name="recall",
    )(state, keys, values, coef)


COMMIT_BLOCK = 4
COMMIT_AHEAD = 3


def commit_kernel(steps, state_ref, unit_ref, writes_ref, whole_ref, out_ref, held_ref, ins, outs):
    seqs, heads, size, _ = held_ref.shape
    span = COMMIT_BLOCK * steps

    def part(ref, step):
        return ref.at[pl.ds(step * COMMIT_BLOCK, COMMIT_BLOCK)]

    def arrive(step):
        return pltpu.make_async_copy(part(state_ref, step), part(held_ref, step), ins.at[step])

    def leave(step):
        return pltpu.make_async_copy(part(held_ref, step), part(out_ref, step), outs.at[step])

    count = seqs // COMMIT_BLOCK
    for step in range(COMMIT_AHEAD):
        arrive(step).start()
    group = lax.broadcasted_iota(jnp.int32, (span, size), 0) // steps

    def body(step, carry):
        base = pl.multiple_of(step * span, span)
        arrive(step).wait()

        @pl.when(step + COMMIT_AHEAD < count)
        def _():
            arrive(step + COMMIT_AHEAD).start()

        for h in range(heads):
            lanes = slice(h * size, (h + 1) * size)
            keys_t = unit_ref[pl.ds(base, span), lanes].astype(F32).T.astype(BF16)
            writes = writes_ref[pl.ds(base, span), lanes].astype(F32)
            whole = whole_ref[pl.ds(base, span), lanes]
            for s in range(0, COMMIT_BLOCK, 2):
                pair = jnp.concatenate(
                    [jnp.where(group == s + i, writes, 0.0).astype(BF16) for i in range(2)], axis=1
                )
                added = jnp.dot(keys_t, pair, preferred_element_type=F32)
                for i in range(2):
                    scale = whole[(s + i) * steps : (s + i) * steps + 1]
                    at = step * COMMIT_BLOCK + s + i
                    held_ref[at, h] = scale * held_ref[at, h] + added[:, i * size : (i + 1) * size]
        leave(step).start()
        return carry

    lax.fori_loop(0, count, body, 0)
    for step in range(count):
        leave(step).wait()


def commit(state, keys, writes, whole, steps):
    count = state.shape[0] // COMMIT_BLOCK
    return pl.pallas_call(
        functools.partial(commit_kernel, steps),
        out_shape=pltpu.HBM(state.shape, F32),
        in_specs=[FAR] + [WHOLE] * 3,
        out_specs=FAR,
        scratch_shapes=[
            pltpu.VMEM(state.shape, F32),
            pltpu.SemaphoreType.DMA((count,)),
            pltpu.SemaphoreType.DMA((count,)),
        ],
        compiler_params=params(16),
        cost_estimate=pl.CostEstimate(flops=4 * 10**9, bytes_accessed=0, transcendentals=0),
        name="commit",
    )(state, keys, writes, whole)


def read_kernel(
    steps,
    core_ref,
    tokens_ref,
    gain_ref,
    query_ref,
    key_ref,
    value_ref,
    gate_ref,
    beta_ref,
    decay_ref,
    log_ref,
    head_gain_ref,
    state_ref,
    unit_ref,
    writes_ref,
    whole_ref,
    out_ref,
    scaled_ref,
    held_ref,
    near_ref,
    sems,
    state_sems,
):
    blocks, rows, width = tokens_ref.shape
    heads, _, size, _ = state_ref.shape
    part = blocks * width // CUTS
    copies = [
        [
            pltpu.make_async_copy(
                ref.at[pl.ds(c * part, part)],
                held_ref.at[i, pl.ds(c * part, part)],
                sems.at[i * CUTS + c],
            )
            for c in range(CUTS)
        ]
        for i, ref in enumerate((query_ref, key_ref, value_ref, gate_ref))
    ]
    states = [
        pltpu.make_async_copy(state_ref.at[h], near_ref.at[h], state_sems.at[h])
        for h in range(heads)
    ]
    queue = [*copies[1], *copies[0], *states, *copies[2], *copies[3]]
    for copy in queue[:READ_AHEAD]:
        copy.start()
    taken = [0]

    def arrive(count):
        for index in range(taken[0], taken[0] + count):
            queue[index].wait()
            if index + READ_AHEAD < len(queue):
                queue[index + READ_AHEAD].start()
        taken[0] += count

    squares = jnp.zeros((rows, width), F32)
    for j in range(blocks):
        wide = tokens_ref[j].astype(F32)
        squares = squares + wide * wide
        scaled_ref[:, j * width : (j + 1) * width] = (wide * gain_ref[j : j + 1]).astype(BF16)
    mean = jnp.sum(squares, axis=1, keepdims=True) / (blocks * width)
    inverse = lax.rsqrt(mean + EPS)
    scaled = scaled_ref[...]
    small = jnp.concatenate([beta_ref[...], decay_ref[...]], axis=0)
    raw = dot_t(scaled, small) * inverse
    every = beta_ref.shape[0]
    lane = lax.broadcasted_iota(jnp.int32, raw.shape, 1)
    first = core_ref[0] * heads

    def column(index):
        picked = jnp.sum(jnp.where(lane == first + index, raw, 0.0), axis=1, keepdims=True)
        return jnp.broadcast_to(picked, (rows, size))

    def project(index):
        raw = jnp.dot(scaled, held_ref[index], preferred_element_type=F32) * inverse
        return [raw[:, h * size : (h + 1) * size] for h in range(heads)]

    row = lax.broadcasted_iota(jnp.int32, (rows, rows), 0)
    col = lax.broadcasted_iota(jnp.int32, (rows, rows), 1)
    same = row // steps == col // steps
    all_heads = range(heads)
    lanes = [slice(h * size, (h + 1) * size) for h in all_heads]
    rates, totals = [], []
    for h in all_heads:
        rates.append(1.0 / (1.0 + jnp.exp(-column(h))))
        lift = column(every + h)
        soft = jnp.maximum(lift, 0.0) + jnp.log1p(jnp.exp(-jnp.abs(lift)))
        totals.append(chain_terms(-jnp.exp(log_ref[:, h : h + 1]) * soft, steps)[0])
    arrive(CUTS)
    keys = [unit(silu(raw)) for raw in project(1)]
    mixes, fades = zip(*(chain_mix(keys[h], rates[h], totals[h], steps) for h in all_heads))
    arrive(CUTS)
    queries = [unit(silu(raw)) * size ** (-0.5) for raw in project(0)]
    weights = [fades[h] * dot_t(queries[h], keys[h]) for h in all_heads]

    def caught_up(left, h):
        recent = jnp.where(same, dot_t(left, unit_ref[:, lanes[h]]), 0.0)
        return dot(recent, writes_ref[:, lanes[h]])

    recents = [(caught_up(keys[h], h), caught_up(queries[h], h)) for h in all_heads]
    arrive(heads)
    recalls, seens = [], []
    for h in all_heads:
        recalled, seen = by_sequence([keys[h], queries[h]], lambda s: near_ref[h, s], steps)
        whole = whole_ref[:, lanes[h]]
        decay = jnp.exp(totals[h])
        recalls.append(rates[h] * decay * (whole * recalled + recents[h][0]))
        seens.append(decay * (whole * seen + recents[h][1]))
    arrive(CUTS)
    reads = []
    for h, raw in enumerate(project(2)):
        writes = chain_writes(mixes[h], rates[h] * silu(raw) - recalls[h])
        value = seens[h] + dot(weights[h], writes)
        mean = jnp.sum(value * value, axis=1, keepdims=True) / size
        reads.append(value * lax.rsqrt(mean + EPS) * head_gain_ref[...])
    arrive(CUTS)
    for h, raw in enumerate(project(3)):
        out_ref[:, lanes[h]] = (reads[h] * silu(raw)).astype(BF16)


def read(core, tokens, gain, weights, beta, decay, decay_log, head_gain, state, kept, steps):
    blocks, rows, width = tokens.shape
    heads, _, size, _ = state.shape
    return pl.pallas_call(
        functools.partial(read_kernel, steps),
        out_shape=VMEM((rows, heads * size), BF16),
        in_specs=[SCALAR] + [WHOLE] * 2 + [FAR] * 4 + [WHOLE] * 4 + [FAR] + [WHOLE] * 3,
        out_specs=WHOLE,
        scratch_shapes=[
            pltpu.VMEM((rows, blocks * width), BF16),
            pltpu.VMEM((4, blocks * width, heads * size), BF16),
            pltpu.VMEM(state.shape, BF16),
            pltpu.SemaphoreType.DMA((4 * CUTS,)),
            pltpu.SemaphoreType.DMA((heads,)),
        ],
        compiler_params=params(24),
        name="read",
    )(core, tokens, gain, *weights, beta, decay, decay_log, head_gain, state, *kept)


def project_kernel(team, *refs):
    *weight_refs, full_ref, send_ref = refs[team:]
    rows = jnp.concatenate([ref[...] for ref in refs[:team]], axis=0)
    for a in range(team):
        for y in range(Y):
            value = dot_t(weight_refs[y][a], rows)
            full_ref[a * Y + y] = value
            send_ref[a * Y + y] = value.astype(BF16)


def project(parts, weights):
    pairs, cols, _ = weights[0].shape
    shape = (pairs * len(weights), cols, len(parts) * parts[0].shape[0])
    return pl.pallas_call(
        functools.partial(project_kernel, len(parts)),
        out_shape=(VMEM(shape, F32), VMEM(shape, BF16)),
        in_specs=[WHOLE] * (len(parts) + len(weights)),
        out_specs=(WHOLE,) * 2,
        compiler_params=params(8),
        name="project",
    )(*parts, *weights)


def combine_kernel(core_ref, mine_ref, other_ref, sum_ref, square_ref):
    blocks, cols, rows = mine_ref.shape
    half = cols // 2
    squares = jnp.zeros((8, rows), F32)
    for j in range(blocks):
        value = mine_ref[j] + other_ref[j].astype(F32)
        squares = squares + jnp.sum((value * value).reshape(cols // 8, 8, rows), axis=0)
    square_ref[...] = squares
    own = pl.ds(pl.multiple_of(core_ref[0] * half, half), half)
    for j in range(blocks):
        sum_ref[j] = mine_ref[j, own, :] + other_ref[j, own, :].astype(F32)


def combine(core, mine, other):
    blocks, cols, rows = mine.shape
    return pl.pallas_call(
        combine_kernel,
        out_shape=(VMEM((blocks, cols // 2, rows), F32), VMEM((8, rows), F32)),
        in_specs=[SCALAR, WHOLE, WHOLE],
        out_specs=(WHOLE,) * 2,
        compiler_params=params(8),
        name="combine",
    )(core, mine, other)


def normalize_kernel(team, model, place_ref, sum_ref, *refs):
    out_ref = refs[team]
    blocks, _, rows = sum_ref.shape
    span = rows // team
    factors = []
    for e in range(team):
        total = 0.0
        for f in range(team):
            part = refs[f][:, (e ^ f) * span : ((e ^ f) + 1) * span]
            total = total + jnp.sum(part, axis=0, keepdims=True)
        factors.append(lax.rsqrt(total / model + EPS))
    factor = jnp.concatenate(factors, axis=1)
    for j in range(blocks):
        out_ref[jnp.bitwise_xor(place_ref[0], j)] = (sum_ref[j] * factor).astype(BF16)


def normalize(place, sums, squares, model):
    return pl.pallas_call(
        functools.partial(normalize_kernel, len(squares), model),
        out_shape=VMEM(sums.shape, BF16),
        in_specs=[SCALAR] + [WHOLE] * (1 + len(squares)),
        out_specs=WHOLE,
        compiler_params=params(8),
        name="normalize",
    )(place, sums, *squares)


def spread_kernel(team, depth_ref, value_ref, gain_ref, out_ref):
    blocks, _, rows = value_ref.shape
    span = rows // team
    gain = gain_ref[...]
    depth = depth_ref[0]
    for m in range(blocks):
        sender = (m // Y) * team + depth % team if team < Y else depth
        value = value_ref[m].astype(F32) * gain
        for e in range(team):
            source = jnp.bitwise_xor(sender, e) * Y + m % Y
            lanes = pl.ds(pl.multiple_of(source * span, span), span)
            out_ref[:, lanes] = value[:, e * span : (e + 1) * span].astype(BF16)


def spread(depth, value, gain, team):
    blocks, cols, rows = value.shape
    return pl.pallas_call(
        functools.partial(spread_kernel, team),
        out_shape=jax.ShapeDtypeStruct((cols, blocks * rows), BF16),
        in_specs=[SCALAR, WHOLE, WHOLE],
        compiler_params=params(8),
        name="spread",
    )(depth, value, gain)


def layer(
    tokens,
    pre_gain,
    query_weight,
    key_weight,
    value_weight,
    gate_weight,
    beta_weight,
    decay_weight,
    decay_log,
    head_gain,
    out_weight,
    post_gain,
    saved_state,
    earlier_keys,
    earlier_values,
    earlier_rates,
    earlier_decays,
    accepted,
):
    seqs, heads, size, _ = saved_state.shape
    steps = earlier_keys.shape[1]
    rows = seqs * steps
    model = pre_gain.shape[0]
    groups = lax.axis_size("kv")
    deep = groups // Y
    core = lax.axis_index("tp").reshape(1)
    depth = (lax.axis_index("kv") // Y).reshape(1)
    place = (depth // TEAM) * Y + lax.axis_index("kv") % Y
    swap = [(0, 1), (1, 0)]
    members = [
        [z * Y + y for z in range(first, deep, TEAM) for y in range(Y)] for first in range(TEAM)
    ]

    def shift(value, mask):
        return lax.ppermute(value, "kv", [(k, k ^ mask) for k in range(groups)])

    flipped = out_weight.T
    across = shift(flipped, TEAM * Y)
    own = lax.all_to_all(
        tokens.reshape(groups, rows, tokens.shape[1]), "kv", 0, 0, tiled=True
    )
    two = jnp.stack([flipped, across])
    wide = []
    for y in range(1, Y):
        wide.append(near(shift(two, y)))
    live = jnp.arange(steps)[None, :, None] < accepted[:, None, None]
    coef = jnp.concatenate(
        [jnp.where(live, earlier_rates, 0.0), jnp.where(live, earlier_decays, 0.0)], axis=2
    ).reshape(rows, 2 * heads)
    state, *kept = recall(
        far(saved_state),
        near(earlier_keys.reshape(rows, heads * size)),
        near(earlier_values.reshape(rows, heads * size)),
        near(coef),
        steps,
    )
    state = far(state)
    kept = tuple(near(value) for value in kept)
    attended = read(
        core,
        near(own),
        near(pre_gain.reshape(groups, -1)),
        tuple(far(w) for w in (query_weight, key_weight, value_weight, gate_weight)),
        near(beta_weight.T),
        near(decay_weight.T),
        near(decay_log.reshape(1, heads)),
        near(head_gain.reshape(1, size)),
        state,
        kept,
        steps,
    )
    parts = [attended] + [shift(attended, e * Y) for e in range(1, TEAM)]
    full, send = project([near(part) for part in parts], [near(two), *wide])
    other = lax.ppermute(send, "tp", swap)
    sums, squares = combine(core, near(full), near(other))
    squares = [squares] + [shift(squares, e * Y) for e in range(1, TEAM)]
    packed = normalize(place, near(sums), [near(part) for part in squares], model)
    arrived = lax.all_to_all(packed, "kv", 0, 0, axis_index_groups=members, tiled=True)
    committed = commit(far(saved_state), *kept, steps)
    mixed = spread(depth, near(arrived), near(post_gain.reshape(-1, 1)), TEAM).T
    return (mixed, committed)


def solution(mesh):
    placed = (
        P("dp", "kv"),
        P(),
        P(None, "tp"),
        P(None, "tp"),
        P(None, "tp"),
        P(None, "tp"),
        P(),
        P(),
        P("tp"),
        P(),
        P("tp", "kv"),
        P(("kv", "tp")),
        P(("dp", "kv"), "tp", None, None),
        P(("dp", "kv"), None, "tp", None),
        P(("dp", "kv"), None, "tp", None),
        P(("dp", "kv"), None, "tp"),
        P(("dp", "kv"), None, "tp"),
        P(("dp", "kv")),
    )
    return jax.shard_map(
        layer,
        mesh=mesh,
        in_specs=placed,
        out_specs=(P("dp", ("kv", "tp")), P(("dp", "kv"), "tp", None, None)),
        check_vma=False,
    )
```

time: 83.3 us -> 66.8 us (0.80)
  the two profiles are of different devices: /device:TPU:1 before, /device:TPU:0 now
where the time goes in v2:
time: 66.8 us; the launch traced here: 66.4 us
  Pallas kernels  23.3 us (35%)
  starting transfers between devices  22.2 us (33%)
  waiting for transfers between devices  16.5 us (25%)
  local copies, waits for them, and re-layouts  2.22 us (3%)
  other arithmetic  1.42 us (2%)
  between operations  0.81 us (1%)
    ppermute x6, waiting for transfers between devices, shift(): return lax.ppermute(value, 'kv', [(k, k ^ mask) for k in range(groups)])  13 us
    ppermute x6, starting transfers between devices, shift(): return lax.ppermute(value, 'kv', [(k, k ^ mask) for k in range(groups)])  9.83 us
    all_to_all x1, starting transfers between devices, layer(): lax.all_to_all(tokens.reshape(groups, rows, tokens.shape[1]), 'kv', 0, 0,...  8.17 us
    pallas_call x1, Pallas kernels, read(): pl.pallas_call(functools.partial(read_kernel, steps), out_shape=VMEM((row...  7.38 us
    pallas_call x1, Pallas kernels, commit(): pl.pallas_call(functools.partial(commit_kernel, steps), out_shape=pltpu.H...  7.14 us
    pallas_call x1, Pallas kernels, recall(): pl.pallas_call(functools.partial(recall_kernel, steps), out_shape=(pltpu....  6.22 us
    all_to_all x1, starting transfers between devices, layer(): lax.all_to_all(packed, 'kv', 0, 0, axis_index_groups=members, tiled=True)  4.07 us
    ppermute x1, waiting for transfers between devices, layer(): other = lax.ppermute(send, 'tp', swap)  1.9 us
  transfers between devices with their start and end apart: 9, of which 5 were waited for; matrix products, arithmetic and copies ran while one was open for 5% of the time, Pallas kernels for 31%

profile of v2, /device:TPU:0, one launch (start us, length us, event | category | flops | bytes accessed | tf_op | source)
XLA Modules:
  0.0 66.4 jit_solution(4327967368956475868)
XLA Ops:
  0.6 8.2 %all-to-all-start = ((bf16[16,128,128]{2,1,0:T(8,128)(2,1)}), bf16[16,128,128]{2,1,0:T(8,128)(2,1)S(1)}, u32[]{:S(2)}, u32[]{:S(2)}) async-start(bf16[16,128,128]{2,1,0:T(8,128)(2,1)} %bitcast.30), calls=%async_computation | async-start | bytes 1048576 | tf_op jit(solution)/shard_map/all_to_all | solution.py:534
  8.8 1.0 %copy.21 = bf16[512,128]{0,1:T(8,128)(2,1)S(1)} copy(bf16[512,128]{1,0:T(8,128)(2,1)} %param.28) | data formatting | bytes 262144 | tf_op args[10]
  9.8 3.5 %collective-permute-start.1 = (bf16[128,512]{1,0:T(8,128)(2,1)S(1)}, bf16[128,512]{1,0:T(8,128)(2,1)S(1)}, u32[]{:S(2)}, u32[]{:S(2)}) collective-permute-start(bf16[128,512]{1,0:T(8,128)(2,1)S(1)} %bitcast.31), channel_id=1, source_target_pairs={{0,16},{2,18},{4,20},{6,22},{8,24},{10,26},{12,28},{14,30},{16,0},... | collective-permute-start | bytes 393224 | tf_op jit(solution)/shard_map/ppermute | solution.py:530
  13.3 0.7 iota_compare_fusion
  14.0 0.7 %broadcast_select_fusion.1 = (f32[32,4,4]{0,2,1:T(4,128)S(1)}, f32[32,4,4]{0,2,1:T(4,128)S(1)}) fusion(f32[32,4,4]{0,2,1:T(4,128)} %param.33, pred[32,4]{0,1:T(4,128)(4,1)S(1)} %iota_compare_fusion, f32[32,4,4]{0,2,1:T(4,128)} %param.34), kind=kLoop, calls=%fused_computation.5 | loop fusion | flops 1024 | bytes 8320 | tf_op jit(solution)/shard_map/jit(_where)/select_n | solution.py:543
  14.7 0.1 copy.20
  14.8 6.5 %collective-permute-done.1 = bf16[128,512]{1,0:T(8,128)(2,1)S(1)} collective-permute-done((bf16[128,512]{1,0:T(8,128)(2,1)S(1)}, bf16[128,512]{1,0:T(8,128)(2,1)S(1)}, u32[]{:S(2)}, u32[]{:S(2)}) %collective-permute-start.1) | collective-permute-done | bytes 131104 | tf_op jit(solution)/shard_map/ppermute | solution.py:530
  21.3 2.5 %collective-permute-start.4 = (bf16[2,128,512]{2,1,0:T(8,128)(2,1)S(1)}, bf16[2,128,512]{2,1,0:T(8,128)(2,1)S(1)}, u32[]{:S(2)}, u32[]{:S(2)}) collective-permute-start(bf16[2,128,512]{2,1,0:T(8,128)(2,1)S(1)} %pad_maximum_fusion.refs_2_), channel_id=1, source_target_pairs={{0,6},{2,4},{4,2},{6,0},{8,14},{10,12},{12,10},{14,8},{16,22},{18,... | collective-permute-start | bytes 786440 | tf_op jit(solution)/shard_map/ppermute | solution.py:530
  23.8 1.1 %collective-permute-start.3 = (bf16[2,128,512]{2,1,0:T(8,128)(2,1)S(1)}, bf16[2,128,512]{2,1,0:T(8,128)(2,1)S(1)}, u32[]{:S(2)}, u32[]{:S(2)}) collective-permute-start(bf16[2,128,512]{2,1,0:T(8,128)(2,1)S(1)} %pad_maximum_fusion.refs_2_), channel_id=1, source_target_pairs={{0,4},{2,6},{4,0},{6,2},{8,12},{10,14},{12,8},{14,10},{16,20},{18,... | collective-permute-start | bytes 786440 | tf_op jit(solution)/shard_map/ppermute | solution.py:530
  24.8 0.6 collective-permute-start.2
  25.5 1.0 %copy_bitcast_fusion = (bf16[128,512]{1,0:T(8,128)(2,1)S(1)}, bf16[128,512]{1,0:T(8,128)(2,1)S(1)}) fusion(bf16[16,8,4,128]{3,2,1,0:T(4,128)(2,1)} %bitcast.34, bf16[16,8,4,128]{3,2,1,0:T(4,128)(2,1)} %bitcast.35), kind=kLoop, calls=%fused_computation.1 | loop fusion | bytes 524288 | tf_op jit(solution)/shard_map/reshape | solution.py:548
  26.5 0.0 copy-start
  26.5 0.0 copy-start.1
  26.5 0.0 copy-start.2
  26.5 0.0 copy-start.3
  26.5 0.0 copy-start.4
  26.5 6.2 %recall.1 = (bf16[4,32,128,128]{3,2,1,0:T(8,128)(2,1)}, bf16[128,512]{1,0:T(8,128)(2,1)S(1)}, bf16[128,512]{1,0:T(8,128)(2,1)S(1)}, f32[128,512]{1,0:T(8,128)S(1)}) custom-call(f32[32,4,128,128]{3,2,1,0:T(8,128)} %state_ref.1, bf16[128,512]{1,0:T(8,128)(2,1)S(1)} %get-tuple-element.21.keys_ref, bf16[128,512]{1,0:T(8,128)(2,1)S(1)} %get-tuple-element.20.values_ref, ...), custom_call_target="tpu_custom_call" | custom-call | tf_op jit(solution)/shard_map/recall/pallas_call | solution.py:165
  32.8 0.0 all-to-all-done.tokens_ref
  32.8 0.0 copy-done
  32.8 0.0 copy-done.1
  32.8 0.0 copy-done.2
  32.8 0.0 copy-done.3
  32.8 0.0 copy-done.4
  32.8 7.4 %read.1.refs_0_ = bf16[128,512]{1,0:T(8,128)(2,1)S(1)} custom-call(s32[1]{0:T(128)} %bitcast.2.core_ref, bf16[16,128,128]{2,1,0:T(8,128)(2,1)S(1)} %all-to-all-done.tokens_ref, f32[16,128]{1,0:T(8,128)S(1)} %bitcast.27, bf16[2048,512]{1,0:T(8,128)(2,1)} %query_ref.1, bf16[2048,512]{1,0:T(8,128)(2,1)} %key_ref.1, bf16[2048,512]{1,0:T(8,128)(2,1)} %value_ref.1, ...), custom_call_target="tpu_custom_call" | custom-call | tf_op jit(solution)/shard_map/read/pallas_call | solution.py:378
  40.2 0.0 copy-start.5
  40.2 1.1 %collective-permute-start = (bf16[128,512]{1,0:T(8,128)(2,1)S(1)}, bf16[128,512]{1,0:T(8,128)(2,1)S(1)}, u32[]{:S(2)}, u32[]{:S(2)}) collective-permute-start(bf16[128,512]{1,0:T(8,128)(2,1)S(1)} %read.1.refs_0_), channel_id=1, source_target_pairs={{0,8},{2,10},{4,12},{6,14},{8,0},{10,2},{12,4},{14,6},{16,24},{18,... | collective-permute-start | bytes 393224 | tf_op jit(solution)/shard_map/ppermute | solution.py:530
  41.3 0.0 collective-permute-done.4.refs_5_
  41.3 0.0 collective-permute-done.3.refs_4_
  41.3 0.0 collective-permute-done.2.refs_3_
  41.3 4.0 %collective-permute-done.refs_1_ = bf16[128,512]{1,0:T(8,128)(2,1)S(1)} collective-permute-done((bf16[128,512]{1,0:T(8,128)(2,1)S(1)}, bf16[128,512]{1,0:T(8,128)(2,1)S(1)}, u32[]{:S(2)}, u32[]{:S(2)}) %collective-permute-start) | collective-permute-done | bytes 131104 | tf_op jit(solution)/shard_map/ppermute | solution.py:530
  45.3 0.8 %project.1 = (f32[8,128,256]{2,1,0:T(8,128)S(1)}, bf16[8,128,256]{2,1,0:T(8,128)(2,1)S(1)}) custom-call(bf16[128,512]{1,0:T(8,128)(2,1)S(1)} %read.1.refs_0_, bf16[128,512]{1,0:T(8,128)(2,1)S(1)} %collective-permute-done.refs_1_, bf16[2,128,512]{2,1,0:T(8,128)(2,1)S(1)} %pad_maximum_fusion.refs_2_, bf16[2,128,512]{2,1,0:T(8,128)(2,1)S(1)} %collective-permute-done.2.refs_3_, ...), custom_call_target="tpu_custom_call" | custom-call | tf_op jit(solution)/shard_map/project/pallas_call | solution.py:408
  46.1 0.1 collective-permute-start.5
  46.2 1.9 %collective-permute-done.5.other_ref = bf16[8,128,256]{2,1,0:T(8,128)(2,1)S(1)} collective-permute-done((bf16[8,128,256]{2,1,0:T(8,128)(2,1)S(1)}, bf16[8,128,256]{2,1,0:T(8,128)(2,1)S(1)}, u32[]{:S(2)}, u32[]{:S(2)}) %collective-permute-start.5) | collective-permute-done | bytes 524320 | tf_op jit(solution)/shard_map/ppermute | solution.py:569
  48.1 0.2 combine.1
  48.2 1.1 %collective-permute-start.6 = (f32[8,256]{1,0:T(8,128)S(1)}, f32[8,256]{1,0:T(8,128)S(1)}, u32[]{:S(2)}, u32[]{:S(2)}) collective-permute-start(f32[8,256]{1,0:T(8,128)S(1)} %get-tuple-element.17.refs_0_), channel_id=1, source_target_pairs={{0,8},{2,10},{4,12},{6,14},{8,0},{10,2},{12,4},{14,6},{16,24},{18,... | collective-permute-start | bytes 24584 | tf_op jit(solution)/shard_map/ppermute | solution.py:530
  49.3 0.0 copy-done.5
  49.3 0.1 copy.22.gain_ref
  49.4 2.6 %collective-permute-done.6.refs_1_ = f32[8,256]{1,0:T(8,128)S(1)} collective-permute-done((f32[8,256]{1,0:T(8,128)S(1)}, f32[8,256]{1,0:T(8,128)S(1)}, u32[]{:S(2)}, u32[]{:S(2)}) %collective-permute-start.6) | collective-permute-done | bytes 8224 | tf_op jit(solution)/shard_map/ppermute | solution.py:530
  52.0 0.7 %normalize.1 = bf16[8,64,256]{2,1,0:T(8,128)(2,1)} custom-call(s32[1]{0:T(128)S(6)} %add.14.place_ref, f32[8,64,256]{2,1,0:T(8,128)S(1)} %get-tuple-element.16.sum_ref, f32[8,256]{1,0:T(8,128)S(1)} %get-tuple-element.17.refs_0_, f32[8,256]{1,0:T(8,128)S(1)} %collective-permute-done.6.refs_1_), custom_call_target="tpu_custom_call" | custom-call | tf_op jit(solution)/shard_map/normalize/pallas_call | solution.py:460
  52.7 4.1 %all-to-all-start.1 = ((bf16[8,64,256]{2,1,0:T(8,128)(2,1)}), bf16[8,64,256]{2,1,0:T(8,128)(2,1)S(1)}, u32[]{:S(2)}, u32[]{:S(2)}) async-start(bf16[8,64,256]{2,1,0:T(8,128)(2,1)} %normalize.1), calls=%async_computation.1 | async-start | bytes 524288 | tf_op jit(solution)/shard_map/all_to_all | solution.py:573
  56.8 7.1 %commit.1 = f32[32,4,128,128]{3,2,1,0:T(8,128)} custom-call(f32[32,4,128,128]{3,2,1,0:T(8,128)} %state_ref.1, bf16[128,512]{1,0:T(8,128)(2,1)S(1)} %get-tuple-element.11.unit_ref, bf16[128,512]{1,0:T(8,128)(2,1)S(1)} %get-tuple-element.12.writes_ref, f32[128,512]{1,0:T(8,128)S(1)} %get-tuple-element.13.whole_ref), custom_call_target="tpu_custom_call" | custom-call | flops 4000000000 | tf_op jit(solution)/shard_map/commit/pallas_call | solution.py:240
  63.9 1.6 %all-to-all-done.1.value_ref = bf16[8,64,256]{2,1,0:T(8,128)(2,1)S(1)} async-done(((bf16[8,64,256]{2,1,0:T(8,128)(2,1)}), bf16[8,64,256]{2,1,0:T(8,128)(2,1)S(1)}, u32[]{:S(2)}, u32[]{:S(2)}) %all-to-all-start.1) | async-done | bytes 262176 | tf_op jit(solution)/shard_map/all_to_all | solution.py:573
  65.6 0.8 %spread.1 = bf16[64,2048]{1,0:T(8,128)(2,1)} custom-call(s32[1]{0:T(128)} %bitcast.depth_ref, bf16[8,64,256]{2,1,0:T(8,128)(2,1)S(1)} %all-to-all-done.1.value_ref, f32[64,1]{1,0:T(8,128)S(1)} %copy.22.gain_ref), custom_call_target="tpu_custom_call" | custom-call | tf_op jit(solution)/shard_map/spread/pallas_call | solution.py:486
  (2 shorter events, 0.0 us)
Async XLA Ops:
  0.6 32.1 %all-to-all-start = ((bf16[16,128,128]{2,1,0:T(8,128)(2,1)}), bf16[16,128,128]{2,1,0:T(8,128)(2,1)S(1)}, u32[]{:S(2)}, u32[]{:S(2)}) async-start(bf16[16,128,128]{2,1,0:T(8,128)(2,1)} %bitcast.30), calls=%async_computation | async-start | bytes 1048576 | tf_op jit(solution)/shard_map/all_to_all | solution.py:534
  9.8 11.5 %collective-permute-start.1 = (bf16[128,512]{1,0:T(8,128)(2,1)S(1)}, bf16[128,512]{1,0:T(8,128)(2,1)S(1)}, u32[]{:S(2)}, u32[]{:S(2)}) collective-permute-start(bf16[128,512]{1,0:T(8,128)(2,1)S(1)} %bitcast.31), channel_id=1, source_target_pairs={{0,16},{2,18},{4,20},{6,22},{8,24},{10,26},{12,28},{14,30},{16,0},... | collective-permute-start | bytes 393224 | tf_op jit(solution)/shard_map/ppermute | solution.py:530
  21.3 20.0 %collective-permute-start.4 = (bf16[2,128,512]{2,1,0:T(8,128)(2,1)S(1)}, bf16[2,128,512]{2,1,0:T(8,128)(2,1)S(1)}, u32[]{:S(2)}, u32[]{:S(2)}) collective-permute-start(bf16[2,128,512]{2,1,0:T(8,128)(2,1)S(1)} %pad_maximum_fusion.refs_2_), channel_id=1, source_target_pairs={{0,6},{2,4},{4,2},{6,0},{8,14},{10,12},{12,10},{14,8},{16,22},{18,... | collective-permute-start | bytes 786440 | tf_op jit(solution)/shard_map/ppermute | solution.py:530
  23.8 17.5 %collective-permute-start.3 = (bf16[2,128,512]{2,1,0:T(8,128)(2,1)S(1)}, bf16[2,128,512]{2,1,0:T(8,128)(2,1)S(1)}, u32[]{:S(2)}, u32[]{:S(2)}) collective-permute-start(bf16[2,128,512]{2,1,0:T(8,128)(2,1)S(1)} %pad_maximum_fusion.refs_2_), channel_id=1, source_target_pairs={{0,4},{2,6},{4,0},{6,2},{8,12},{10,14},{12,8},{14,10},{16,20},{18,... | collective-permute-start | bytes 786440 | tf_op jit(solution)/shard_map/ppermute | solution.py:530
  24.8 16.5 %collective-permute-start.2 = (bf16[2,128,512]{2,1,0:T(8,128)(2,1)S(1)}, bf16[2,128,512]{2,1,0:T(8,128)(2,1)S(1)}, u32[]{:S(2)}, u32[]{:S(2)}) collective-permute-start(bf16[2,128,512]{2,1,0:T(8,128)(2,1)S(1)} %pad_maximum_fusion.refs_2_), channel_id=1, source_target_pairs={{0,2},{2,0},{4,6},{6,4},{8,10},{10,8},{12,14},{14,12},{16,18},{18,... | collective-permute-start | bytes 786440 | tf_op jit(solution)/shard_map/ppermute | solution.py:530
  26.5 6.3 %copy-start = (bf16[2048,8]{0,1:T(8,128)(2,1)S(1)}, bf16[2048,8]{0,1:T(8,128)(2,1)}, u32[]{:S(2)}) copy-start(bf16[2048,8]{0,1:T(8,128)(2,1)} %param.24) | copy-start | bytes 98308
  26.5 6.3 %copy-start.1 = (bf16[2048,8]{0,1:T(8,128)(2,1)S(1)}, bf16[2048,8]{0,1:T(8,128)(2,1)}, u32[]{:S(2)}) copy-start(bf16[2048,8]{0,1:T(8,128)(2,1)} %param.25) | copy-start | bytes 98308
  26.5 6.3 %copy-start.2 = (f32[2048]{0:T(1024)S(1)}, f32[2048]{0:T(1024)}, u32[]{:S(2)}) copy-start(f32[2048]{0:T(1024)} %param.19) | copy-start | bytes 24580
  26.5 6.3 %copy-start.3 = (f32[4]{0:T(128)S(1)}, f32[4]{0:T(128)}, u32[]{:S(2)}) copy-start(f32[4]{0:T(128)} %param.26) | copy-start | bytes 52
  26.5 6.3 %copy-start.4 = (f32[128]{0:T(128)S(1)}, f32[128]{0:T(128)}, u32[]{:S(2)}) copy-start(f32[128]{0:T(128)} %param.27) | copy-start | bytes 1540
  40.2 9.1 %copy-start.5 = (f32[64]{0:T(128)S(1)}, f32[64]{0:T(128)}, u32[]{:S(2)}) copy-start(f32[64]{0:T(128)} %param.29) | copy-start | bytes 772
  40.2 5.0 %collective-permute-start = (bf16[128,512]{1,0:T(8,128)(2,1)S(1)}, bf16[128,512]{1,0:T(8,128)(2,1)S(1)}, u32[]{:S(2)}, u32[]{:S(2)}) collective-permute-start(bf16[128,512]{1,0:T(8,128)(2,1)S(1)} %read.1.refs_0_), channel_id=1, source_target_pairs={{0,8},{2,10},{4,12},{6,14},{8,0},{10,2},{12,4},{14,6},{16,24},{18,... | collective-permute-start | bytes 393224 | tf_op jit(solution)/shard_map/ppermute | solution.py:530
  46.1 2.0 %collective-permute-start.5 = (bf16[8,128,256]{2,1,0:T(8,128)(2,1)S(1)}, bf16[8,128,256]{2,1,0:T(8,128)(2,1)S(1)}, u32[]{:S(2)}, u32[]{:S(2)}) collective-permute-start(bf16[8,128,256]{2,1,0:T(8,128)(2,1)S(1)} %get-tuple-element.15), channel_id=1, source_target_pairs={{0,1},{1,0},{2,3},{3,2},{4,5},{5,4},{6,7},{7,6},{8,9},{9,8},{10,11... | collective-permute-start | bytes 1572872 | tf_op jit(solution)/shard_map/ppermute | solution.py:569
  48.2 3.7 %collective-permute-start.6 = (f32[8,256]{1,0:T(8,128)S(1)}, f32[8,256]{1,0:T(8,128)S(1)}, u32[]{:S(2)}, u32[]{:S(2)}) collective-permute-start(f32[8,256]{1,0:T(8,128)S(1)} %get-tuple-element.17.refs_0_), channel_id=1, source_target_pairs={{0,8},{2,10},{4,12},{6,14},{8,0},{10,2},{12,4},{14,6},{16,24},{18,... | collective-permute-start | bytes 24584 | tf_op jit(solution)/shard_map/ppermute | solution.py:530
  52.7 12.9 %all-to-all-start.1 = ((bf16[8,64,256]{2,1,0:T(8,128)(2,1)}), bf16[8,64,256]{2,1,0:T(8,128)(2,1)S(1)}, u32[]{:S(2)}, u32[]{:S(2)}) async-start(bf16[8,64,256]{2,1,0:T(8,128)(2,1)} %normalize.1), calls=%async_computation.1 | async-start | bytes 524288 | tf_op jit(solution)/shard_map/all_to_all | solution.py:573

commit v3 on v2

--- a/solution.py
+++ b/solution.py
@@ -106,13 +106,20 @@
     source_ref,
     keys_ref,
     values_ref,
-    coef_ref,
+    rates_ref,
+    decays_ref,
+    accepted_ref,
     state_ref,
     unit_ref,
     writes_ref,
     whole_ref,
     held_ref,
     short_ref,
+    flat_ref,
+    given_ref,
+    chain_ref,
+    count_ref,
+    small_sems,
     in_sems,
     out_sems,
 ):
@@ -126,20 +133,58 @@
         pltpu.make_async_copy(short_ref.at[h], state_ref.at[h], out_sems.at[h])
         for h in range(heads)
     ]
-    for copy in arrive[:AHEAD]:
+    small = [
+        pltpu.make_async_copy(keys_ref, given_ref.at[0], small_sems.at[0]),
+        pltpu.make_async_copy(values_ref, given_ref.at[1], small_sems.at[1]),
+        pltpu.make_async_copy(rates_ref, chain_ref.at[0], small_sems.at[2]),
+        pltpu.make_async_copy(decays_ref, chain_ref.at[1], small_sems.at[3]),
+        pltpu.make_async_copy(accepted_ref, count_ref, small_sems.at[4]),
+    ]
+    for copy in small + arrive[:AHEAD]:
         copy.start()
+    for copy in small:
+        copy.wait()
+    table = jnp.concatenate(
+        [chain_ref[i, p] for i in range(2) for p in range(steps)]
+        + [jnp.broadcast_to(count_ref[...].astype(F32), (8, seqs))],
+        axis=0,
+    )
+    pick = (
+        lax.broadcasted_iota(jnp.int32, (rows, seqs), 0) // steps
+        == lax.broadcasted_iota(jnp.int32, (rows, seqs), 1)
+    ).astype(F32)
+    spread = lax.dot_general(
+        pick,
+        table,
+        (((1,), (1,)), ((), ())),
+        precision=lax.Precision.HIGHEST,
+        preferred_element_type=F32,
+    )
+    lane = lax.broadcasted_iota(jnp.int32, spread.shape, 1)
+    place = lax.broadcasted_iota(jnp.int32, spread.shape, 0) % steps
+    count = steps * heads
+
+    def column(index):
+        picked = jnp.sum(jnp.where(lane == index, spread, 0.0), axis=1, keepdims=True)
+        return jnp.broadcast_to(picked, (rows, size))
+
+    live = column(2 * count) > place[:, :1].astype(F32)
+
+    def own(first):
+        return jnp.where(live, column(first + place * heads), 0.0)
+
+    for i in range(2):
+        flat_ref[i] = given_ref[i].astype(F32).reshape(rows * heads, size)
     ready = []
     for h in range(heads):
         lanes = slice(h * size, (h + 1) * size)
-        keys = unit(keys_ref[:, lanes].astype(F32))
-        rates = jnp.broadcast_to(coef_ref[:, h : h + 1], (rows, size))
-        total, rest = chain_terms(
-            jnp.broadcast_to(coef_ref[:, heads + h : heads + h + 1], (rows, size)), steps
-        )
+        keys = unit(flat_ref[0, pl.ds(h, rows, heads), :])
+        rates = own(h)
+        total, rest = chain_terms(own(count + h), steps)
         mix, _ = chain_mix(keys, rates, total, steps)
         unit_ref[:, lanes] = keys.astype(BF16)
         whole_ref[:, lanes] = jnp.exp(total + rest)
-        given = rates * values_ref[:, lanes].astype(F32)
+        given = rates * flat_ref[1, pl.ds(h, rows, heads), :]
         ready.append((keys, mix, given, rates * jnp.exp(total), jnp.exp(rest)))
     starts = []
     for h in range(heads):
@@ -158,9 +203,9 @@
         copy.wait()
 
 
-def recall(state, keys, values, coef, steps):
-    rows, width = keys.shape
+def recall(state, keys, values, rates, decays, accepted, steps):
     seqs, heads, size, _ = state.shape
+    rows, width = seqs * steps, heads * size
     turned = (heads, seqs, size, size)
     return pl.pallas_call(
         functools.partial(recall_kernel, steps),
@@ -170,17 +215,22 @@
             VMEM((rows, width), BF16),
             VMEM((rows, width), F32),
         ),
-        in_specs=[FAR] + [WHOLE] * 3,
+        in_specs=[FAR] * 6,
         out_specs=(FAR,) + (WHOLE,) * 3,
         scratch_shapes=[
             pltpu.VMEM(turned, F32),
             pltpu.VMEM(turned, BF16),
+            pltpu.VMEM((2, rows * heads, size), F32),
+            pltpu.VMEM((2, *keys.shape), BF16),
+            pltpu.VMEM((2, *rates.shape), F32),
+            pltpu.VMEM(accepted.shape, jnp.int32),
+            pltpu.SemaphoreType.DMA((5,)),
             pltpu.SemaphoreType.DMA((heads,)),
             pltpu.SemaphoreType.DMA((heads,)),
         ],
         compiler_params=params(20),
         name="recall",
-    )(state, keys, values, coef)
+    )(state, keys, values, rates, decays, accepted)
 
 
 COMMIT_BLOCK = 4
@@ -538,15 +588,13 @@
     wide = []
     for y in range(1, Y):
         wide.append(near(shift(two, y)))
-    live = jnp.arange(steps)[None, :, None] < accepted[:, None, None]
-    coef = jnp.concatenate(
-        [jnp.where(live, earlier_rates, 0.0), jnp.where(live, earlier_decays, 0.0)], axis=2
-    ).reshape(rows, 2 * heads)
     state, *kept = recall(
         far(saved_state),
-        near(earlier_keys.reshape(rows, heads * size)),
-        near(earlier_values.reshape(rows, heads * size)),
-        near(coef),
+        far(earlier_keys),
+        far(earlier_values),
+        far(earlier_rates.transpose(1, 2, 0)),
+        far(earlier_decays.transpose(1, 2, 0)),
+        far(accepted.reshape(1, seqs)),
         steps,
     )
     state = far(state)

time: 66.8 us -> 65.5 us (0.981)
  waiting for transfers between devices: 16.5 us -> 18 us
  other arithmetic: 1.42 us -> 0.03 us
  local copies, waits for them, and re-layouts: 2.22 us -> 1.13 us
    ppermute x6, waiting for transfers between devices: 13 us -> 14.5 us  [shift(): return lax.ppermute(value, 'kv', [(k, k ^ mask) for k in range(groups)])]
    reshape x1 -> x0, local copies, waits for them, and re-layouts: 1 us -> none  [layer(): earlier_values.reshape(rows, heads * size)]
    select_n x1 -> x0, other arithmetic: 0.72 us -> none  [layer(): jnp.where(live, earlier_rates, 0.0)]
  transfers between devices with their start and end apart: 9 -> 9, of which waited for: 5 -> 5; matrix products, arithmetic and copies ran while one was open for 5% -> 2% of each run, Pallas kernels for 31% -> 31%
where the time goes in v3:
time: 65.5 us; the launch traced here: 65.1 us
  Pallas kernels  23 us (35%)
  starting transfers between devices  22.1 us (34%)
  waiting for transfers between devices  18 us (27%)
  local copies, waits for them, and re-layouts  1.13 us (2%)
  between operations  0.77 us (1%)
    ppermute x6, waiting for transfers between devices, shift(): return lax.ppermute(value, 'kv', [(k, k ^ mask) for k in range(groups)])  14.5 us
    ppermute x6, starting transfers between devices, shift(): return lax.ppermute(value, 'kv', [(k, k ^ mask) for k in range(groups)])  9.81 us
    all_to_all x1, starting transfers between devices, layer(): lax.all_to_all(tokens.reshape(groups, rows, tokens.shape[1]), 'kv', 0, 0,...  8.17 us
    pallas_call x1, Pallas kernels, read(): pl.pallas_call(functools.partial(read_kernel, steps), out_shape=VMEM((row...  7.38 us
    pallas_call x1, Pallas kernels, commit(): pl.pallas_call(functools.partial(commit_kernel, steps), out_shape=pltpu.H...  7.14 us
    pallas_call x1, Pallas kernels, recall(): pl.pallas_call(functools.partial(recall_kernel, steps), out_shape=(pltpu....  5.95 us
    all_to_all x1, starting transfers between devices, layer(): lax.all_to_all(packed, 'kv', 0, 0, axis_index_groups=members, tiled=True)  4.07 us
    ppermute x1, waiting for transfers between devices, layer(): other = lax.ppermute(send, 'tp', swap)  1.9 us
  transfers between devices with their start and end apart: 9, of which 5 were waited for; matrix products, arithmetic and copies ran while one was open for 2% of the time, Pallas kernels for 31%

profile of v3, /device:TPU:0, one launch (start us, length us, event | category | flops | bytes accessed | tf_op | source)
XLA Modules:
  0.0 65.1 jit_solution(2624300518500830127)
XLA Ops:
  0.6 8.2 %all-to-all-start = ((bf16[16,128,128]{2,1,0:T(8,128)(2,1)}), bf16[16,128,128]{2,1,0:T(8,128)(2,1)S(1)}, u32[]{:S(2)}, u32[]{:S(2)}) async-start(bf16[16,128,128]{2,1,0:T(8,128)(2,1)} %bitcast.23), calls=%async_computation | async-start | bytes 1048576 | tf_op jit(solution)/shard_map/all_to_all | solution.py:584
  8.8 1.0 %copy.20 = bf16[512,128]{0,1:T(8,128)(2,1)S(1)} copy(bf16[512,128]{1,0:T(8,128)(2,1)} %param.28) | data formatting | bytes 262144 | tf_op args[10]
  9.8 3.5 %collective-permute-start.1 = (bf16[128,512]{1,0:T(8,128)(2,1)S(1)}, bf16[128,512]{1,0:T(8,128)(2,1)S(1)}, u32[]{:S(2)}, u32[]{:S(2)}) collective-permute-start(bf16[128,512]{1,0:T(8,128)(2,1)S(1)} %bitcast.24), channel_id=1, source_target_pairs={{0,16},{2,18},{4,20},{6,22},{8,24},{10,26},{12,28},{14,30},{16,0},... | collective-permute-start | bytes 393224 | tf_op jit(solution)/shard_map/ppermute | solution.py:580
  13.3 7.9 %collective-permute-done.1 = bf16[128,512]{1,0:T(8,128)(2,1)S(1)} collective-permute-done((bf16[128,512]{1,0:T(8,128)(2,1)S(1)}, bf16[128,512]{1,0:T(8,128)(2,1)S(1)}, u32[]{:S(2)}, u32[]{:S(2)}) %collective-permute-start.1) | collective-permute-done | bytes 131104 | tf_op jit(solution)/shard_map/ppermute | solution.py:580
  21.3 2.5 %collective-permute-start.4 = (bf16[2,128,512]{2,1,0:T(8,128)(2,1)S(1)}, bf16[2,128,512]{2,1,0:T(8,128)(2,1)S(1)}, u32[]{:S(2)}, u32[]{:S(2)}) collective-permute-start(bf16[2,128,512]{2,1,0:T(8,128)(2,1)S(1)} %pad_maximum_fusion.refs_2_), channel_id=1, source_target_pairs={{0,6},{2,4},{4,2},{6,0},{8,14},{10,12},{12,10},{14,8},{16,22},{18,... | collective-permute-start | bytes 786440 | tf_op jit(solution)/shard_map/ppermute | solution.py:580
  23.8 1.1 %collective-permute-start.3 = (bf16[2,128,512]{2,1,0:T(8,128)(2,1)S(1)}, bf16[2,128,512]{2,1,0:T(8,128)(2,1)S(1)}, u32[]{:S(2)}, u32[]{:S(2)}) collective-permute-start(bf16[2,128,512]{2,1,0:T(8,128)(2,1)S(1)} %pad_maximum_fusion.refs_2_), channel_id=1, source_target_pairs={{0,4},{2,6},{4,0},{6,2},{8,12},{10,14},{12,8},{14,10},{16,20},{18,... | collective-permute-start | bytes 786440 | tf_op jit(solution)/shard_map/ppermute | solution.py:580
  24.8 0.6 collective-permute-start.2
  25.5 0.0 copy-start
  25.5 0.0 copy-start.1
  25.5 0.0 copy-start.2
  25.5 0.0 copy-start.3
  25.5 0.0 copy-start.4
  25.5 6.0 %recall.1 = (bf16[4,32,128,128]{3,2,1,0:T(8,128)(2,1)}, bf16[128,512]{1,0:T(8,128)(2,1)S(1)}, bf16[128,512]{1,0:T(8,128)(2,1)S(1)}, f32[128,512]{1,0:T(8,128)S(1)}) custom-call(f32[32,4,128,128]{3,2,1,0:T(8,128)} %state_ref.1, bf16[32,4,4,128]{3,2,1,0:T(4,128)(2,1)} %keys_ref.1, bf16[32,4,4,128]{3,2,1,0:T(4,128)(2,1)} %values_ref.1, f32[4,4,32]{2,1,0:T(4,128)} %bitcast.28, ...), custom_call_target="tpu_custom_call" | custom-call | tf_op jit(solution)/shard_map/recall/pallas_call | solution.py:210
  31.5 0.0 all-to-all-done.tokens_ref
  31.5 0.0 copy-done
  31.5 0.0 copy-done.1
  31.5 0.0 copy-done.2
  31.5 0.0 copy-done.3
  31.5 0.0 copy-done.4
  31.5 7.4 %read.1.refs_0_ = bf16[128,512]{1,0:T(8,128)(2,1)S(1)} custom-call(s32[1]{0:T(128)} %bitcast.2.core_ref, bf16[16,128,128]{2,1,0:T(8,128)(2,1)S(1)} %all-to-all-done.tokens_ref, f32[16,128]{1,0:T(8,128)S(1)} %bitcast.20, bf16[2048,512]{1,0:T(8,128)(2,1)} %query_ref.1, bf16[2048,512]{1,0:T(8,128)(2,1)} %key_ref.1, bf16[2048,512]{1,0:T(8,128)(2,1)} %value_ref.1, ...), custom_call_target="tpu_custom_call" | custom-call | tf_op jit(solution)/shard_map/read/pallas_call | solution.py:428
  38.9 0.0 copy-start.5
  38.9 1.1 %collective-permute-start = (bf16[128,512]{1,0:T(8,128)(2,1)S(1)}, bf16[128,512]{1,0:T(8,128)(2,1)S(1)}, u32[]{:S(2)}, u32[]{:S(2)}) collective-permute-start(bf16[128,512]{1,0:T(8,128)(2,1)S(1)} %read.1.refs_0_), channel_id=1, source_target_pairs={{0,8},{2,10},{4,12},{6,14},{8,0},{10,2},{12,4},{14,6},{16,24},{18,... | collective-permute-start | bytes 393224 | tf_op jit(solution)/shard_map/ppermute | solution.py:580
  40.0 0.0 collective-permute-done.4.refs_5_
  40.0 0.0 collective-permute-done.3.refs_4_
  40.0 0.0 collective-permute-done.2.refs_3_
  40.0 4.0 %collective-permute-done.refs_1_ = bf16[128,512]{1,0:T(8,128)(2,1)S(1)} collective-permute-done((bf16[128,512]{1,0:T(8,128)(2,1)S(1)}, bf16[128,512]{1,0:T(8,128)(2,1)S(1)}, u32[]{:S(2)}, u32[]{:S(2)}) %collective-permute-start) | collective-permute-done | bytes 131104 | tf_op jit(solution)/shard_map/ppermute | solution.py:580
  44.0 0.8 %project.1 = (f32[8,128,256]{2,1,0:T(8,128)S(1)}, bf16[8,128,256]{2,1,0:T(8,128)(2,1)S(1)}) custom-call(bf16[128,512]{1,0:T(8,128)(2,1)S(1)} %read.1.refs_0_, bf16[128,512]{1,0:T(8,128)(2,1)S(1)} %collective-permute-done.refs_1_, bf16[2,128,512]{2,1,0:T(8,128)(2,1)S(1)} %pad_maximum_fusion.refs_2_, bf16[2,128,512]{2,1,0:T(8,128)(2,1)S(1)} %collective-permute-done.2.refs_3_, ...), custom_call_target="tpu_custom_call" | custom-call | tf_op jit(solution)/shard_map/project/pallas_call | solution.py:458
  44.8 0.1 collective-permute-start.5
  44.9 1.9 %collective-permute-done.5.other_ref = bf16[8,128,256]{2,1,0:T(8,128)(2,1)S(1)} collective-permute-done((bf16[8,128,256]{2,1,0:T(8,128)(2,1)S(1)}, bf16[8,128,256]{2,1,0:T(8,128)(2,1)S(1)}, u32[]{:S(2)}, u32[]{:S(2)}) %collective-permute-start.5) | collective-permute-done | bytes 524320 | tf_op jit(solution)/shard_map/ppermute | solution.py:617
  46.8 0.2 combine.1
  46.9 1.1 %collective-permute-start.6 = (f32[8,256]{1,0:T(8,128)S(1)}, f32[8,256]{1,0:T(8,128)S(1)}, u32[]{:S(2)}, u32[]{:S(2)}) collective-permute-start(f32[8,256]{1,0:T(8,128)S(1)} %get-tuple-element.17.refs_0_), channel_id=1, source_target_pairs={{0,8},{2,10},{4,12},{6,14},{8,0},{10,2},{12,4},{14,6},{16,24},{18,... | collective-permute-start | bytes 24584 | tf_op jit(solution)/shard_map/ppermute | solution.py:580
  48.0 0.0 copy-done.5
  48.0 0.1 copy.21.gain_ref
  48.1 2.6 %collective-permute-done.6.refs_1_ = f32[8,256]{1,0:T(8,128)S(1)} collective-permute-done((f32[8,256]{1,0:T(8,128)S(1)}, f32[8,256]{1,0:T(8,128)S(1)}, u32[]{:S(2)}, u32[]{:S(2)}) %collective-permute-start.6) | collective-permute-done | bytes 8224 | tf_op jit(solution)/shard_map/ppermute | solution.py:580
  50.7 0.7 %normalize.1 = bf16[8,64,256]{2,1,0:T(8,128)(2,1)} custom-call(s32[1]{0:T(128)S(6)} %add.14.place_ref, f32[8,64,256]{2,1,0:T(8,128)S(1)} %get-tuple-element.16.sum_ref, f32[8,256]{1,0:T(8,128)S(1)} %get-tuple-element.17.refs_0_, f32[8,256]{1,0:T(8,128)S(1)} %collective-permute-done.6.refs_1_), custom_call_target="tpu_custom_call" | custom-call | tf_op jit(solution)/shard_map/normalize/pallas_call | solution.py:510
  51.4 4.1 %all-to-all-start.1 = ((bf16[8,64,256]{2,1,0:T(8,128)(2,1)}), bf16[8,64,256]{2,1,0:T(8,128)(2,1)S(1)}, u32[]{:S(2)}, u32[]{:S(2)}) async-start(bf16[8,64,256]{2,1,0:T(8,128)(2,1)} %normalize.1), calls=%async_computation.1 | async-start | bytes 524288 | tf_op jit(solution)/shard_map/all_to_all | solution.py:621
  55.5 7.1 %commit.1 = f32[32,4,128,128]{3,2,1,0:T(8,128)} custom-call(f32[32,4,128,128]{3,2,1,0:T(8,128)} %state_ref.1, bf16[128,512]{1,0:T(8,128)(2,1)S(1)} %get-tuple-element.11.unit_ref, bf16[128,512]{1,0:T(8,128)(2,1)S(1)} %get-tuple-element.12.writes_ref, f32[128,512]{1,0:T(8,128)S(1)} %get-tuple-element.13.whole_ref), custom_call_target="tpu_custom_call" | custom-call | flops 4000000000 | tf_op jit(solution)/shard_map/commit/pallas_call | solution.py:290
  62.6 1.6 %all-to-all-done.1.value_ref = bf16[8,64,256]{2,1,0:T(8,128)(2,1)S(1)} async-done(((bf16[8,64,256]{2,1,0:T(8,128)(2,1)}), bf16[8,64,256]{2,1,0:T(8,128)(2,1)S(1)}, u32[]{:S(2)}, u32[]{:S(2)}) %all-to-all-start.1) | async-done | bytes 262176 | tf_op jit(solution)/shard_map/all_to_all | solution.py:621
  64.3 0.8 %spread.1 = bf16[64,2048]{1,0:T(8,128)(2,1)} custom-call(s32[1]{0:T(128)} %bitcast.depth_ref, bf16[8,64,256]{2,1,0:T(8,128)(2,1)S(1)} %all-to-all-done.1.value_ref, f32[64,1]{1,0:T(8,128)S(1)} %copy.21.gain_ref), custom_call_target="tpu_custom_call" | custom-call | tf_op jit(solution)/shard_map/spread/pallas_call | solution.py:536
  (1 shorter events, 0.0 us)
Async XLA Ops:
  0.6 30.8 %all-to-all-start = ((bf16[16,128,128]{2,1,0:T(8,128)(2,1)}), bf16[16,128,128]{2,1,0:T(8,128)(2,1)S(1)}, u32[]{:S(2)}, u32[]{:S(2)}) async-start(bf16[16,128,128]{2,1,0:T(8,128)(2,1)} %bitcast.23), calls=%async_computation | async-start | bytes 1048576 | tf_op jit(solution)/shard_map/all_to_all | solution.py:584
  9.8 11.5 %collective-permute-start.1 = (bf16[128,512]{1,0:T(8,128)(2,1)S(1)}, bf16[128,512]{1,0:T(8,128)(2,1)S(1)}, u32[]{:S(2)}, u32[]{:S(2)}) collective-permute-start(bf16[128,512]{1,0:T(8,128)(2,1)S(1)} %bitcast.24), channel_id=1, source_target_pairs={{0,16},{2,18},{4,20},{6,22},{8,24},{10,26},{12,28},{14,30},{16,0},... | collective-permute-start | bytes 393224 | tf_op jit(solution)/shard_map/ppermute | solution.py:580
  21.3 18.7 %collective-permute-start.4 = (bf16[2,128,512]{2,1,0:T(8,128)(2,1)S(1)}, bf16[2,128,512]{2,1,0:T(8,128)(2,1)S(1)}, u32[]{:S(2)}, u32[]{:S(2)}) collective-permute-start(bf16[2,128,512]{2,1,0:T(8,128)(2,1)S(1)} %pad_maximum_fusion.refs_2_), channel_id=1, source_target_pairs={{0,6},{2,4},{4,2},{6,0},{8,14},{10,12},{12,10},{14,8},{16,22},{18,... | collective-permute-start | bytes 786440 | tf_op jit(solution)/shard_map/ppermute | solution.py:580
  23.8 16.2 %collective-permute-start.3 = (bf16[2,128,512]{2,1,0:T(8,128)(2,1)S(1)}, bf16[2,128,512]{2,1,0:T(8,128)(2,1)S(1)}, u32[]{:S(2)}, u32[]{:S(2)}) collective-permute-start(bf16[2,128,512]{2,1,0:T(8,128)(2,1)S(1)} %pad_maximum_fusion.refs_2_), channel_id=1, source_target_pairs={{0,4},{2,6},{4,0},{6,2},{8,12},{10,14},{12,8},{14,10},{16,20},{18,... | collective-permute-start | bytes 786440 | tf_op jit(solution)/shard_map/ppermute | solution.py:580
  24.8 15.2 %collective-permute-start.2 = (bf16[2,128,512]{2,1,0:T(8,128)(2,1)S(1)}, bf16[2,128,512]{2,1,0:T(8,128)(2,1)S(1)}, u32[]{:S(2)}, u32[]{:S(2)}) collective-permute-start(bf16[2,128,512]{2,1,0:T(8,128)(2,1)S(1)} %pad_maximum_fusion.refs_2_), channel_id=1, source_target_pairs={{0,2},{2,0},{4,6},{6,4},{8,10},{10,8},{12,14},{14,12},{16,18},{18,... | collective-permute-start | bytes 786440 | tf_op jit(solution)/shard_map/ppermute | solution.py:580
  25.5 6.0 %copy-start = (bf16[2048,8]{0,1:T(8,128)(2,1)S(1)}, bf16[2048,8]{0,1:T(8,128)(2,1)}, u32[]{:S(2)}) copy-start(bf16[2048,8]{0,1:T(8,128)(2,1)} %param.24) | copy-start | bytes 98308
  25.5 6.0 %copy-start.1 = (bf16[2048,8]{0,1:T(8,128)(2,1)S(1)}, bf16[2048,8]{0,1:T(8,128)(2,1)}, u32[]{:S(2)}) copy-start(bf16[2048,8]{0,1:T(8,128)(2,1)} %param.25) | copy-start | bytes 98308
  25.5 6.0 %copy-start.2 = (f32[2048]{0:T(1024)S(1)}, f32[2048]{0:T(1024)}, u32[]{:S(2)}) copy-start(f32[2048]{0:T(1024)} %param.19) | copy-start | bytes 24580
  25.5 6.0 %copy-start.3 = (f32[4]{0:T(128)S(1)}, f32[4]{0:T(128)}, u32[]{:S(2)}) copy-start(f32[4]{0:T(128)} %param.26) | copy-start | bytes 52
  25.5 6.0 %copy-start.4 = (f32[128]{0:T(128)S(1)}, f32[128]{0:T(128)}, u32[]{:S(2)}) copy-start(f32[128]{0:T(128)} %param.27) | copy-start | bytes 1540
  38.9 9.1 %copy-start.5 = (f32[64]{0:T(128)S(1)}, f32[64]{0:T(128)}, u32[]{:S(2)}) copy-start(f32[64]{0:T(128)} %param.29) | copy-start | bytes 772
  38.9 5.0 %collective-permute-start = (bf16[128,512]{1,0:T(8,128)(2,1)S(1)}, bf16[128,512]{1,0:T(8,128)(2,1)S(1)}, u32[]{:S(2)}, u32[]{:S(2)}) collective-permute-start(bf16[128,512]{1,0:T(8,128)(2,1)S(1)} %read.1.refs_0_), channel_id=1, source_target_pairs={{0,8},{2,10},{4,12},{6,14},{8,0},{10,2},{12,4},{14,6},{16,24},{18,... | collective-permute-start | bytes 393224 | tf_op jit(solution)/shard_map/ppermute | solution.py:580
  44.8 2.0 %collective-permute-start.5 = (bf16[8,128,256]{2,1,0:T(8,128)(2,1)S(1)}, bf16[8,128,256]{2,1,0:T(8,128)(2,1)S(1)}, u32[]{:S(2)}, u32[]{:S(2)}) collective-permute-start(bf16[8,128,256]{2,1,0:T(8,128)(2,1)S(1)} %get-tuple-element.15), channel_id=1, source_target_pairs={{0,1},{1,0},{2,3},{3,2},{4,5},{5,4},{6,7},{7,6},{8,9},{9,8},{10,11... | collective-permute-start | bytes 1572872 | tf_op jit(solution)/shard_map/ppermute | solution.py:617
  46.9 3.7 %collective-permute-start.6 = (f32[8,256]{1,0:T(8,128)S(1)}, f32[8,256]{1,0:T(8,128)S(1)}, u32[]{:S(2)}, u32[]{:S(2)}) collective-permute-start(f32[8,256]{1,0:T(8,128)S(1)} %get-tuple-element.17.refs_0_), channel_id=1, source_target_pairs={{0,8},{2,10},{4,12},{6,14},{8,0},{10,2},{12,4},{14,6},{16,24},{18,... | collective-permute-start | bytes 24584 | tf_op jit(solution)/shard_map/ppermute | solution.py:580
  51.4 12.9 %all-to-all-start.1 = ((bf16[8,64,256]{2,1,0:T(8,128)(2,1)}), bf16[8,64,256]{2,1,0:T(8,128)(2,1)S(1)}, u32[]{:S(2)}, u32[]{:S(2)}) async-start(bf16[8,64,256]{2,1,0:T(8,128)(2,1)} %normalize.1), calls=%async_computation.1 | async-start | bytes 524288 | tf_op jit(solution)/shard_map/all_to_all | solution.py:621

commit v4 on v3

--- a/solution.py
+++ b/solution.py
@@ -447,13 +447,13 @@
     rows = jnp.concatenate([ref[...] for ref in refs[:team]], axis=0)
     for a in range(team):
         for y in range(Y):
-            value = dot_t(weight_refs[y][a], rows)
+            value = dot(rows, weight_refs[y][a]).T
             full_ref[a * Y + y] = value
             send_ref[a * Y + y] = value.astype(BF16)
 
 
 def project(parts, weights):
-    pairs, cols, _ = weights[0].shape
+    pairs, _, cols = weights[0].shape
     shape = (pairs * len(weights), cols, len(parts) * parts[0].shape[0])
     return pl.pallas_call(
         functools.partial(project_kernel, len(parts)),
@@ -579,7 +579,7 @@
     def shift(value, mask):
         return lax.ppermute(value, "kv", [(k, k ^ mask) for k in range(groups)])
 
-    flipped = out_weight.T
+    flipped = out_weight
     across = shift(flipped, TEAM * Y)
     own = lax.all_to_all(
         tokens.reshape(groups, rows, tokens.shape[1]), "kv", 0, 0, tiled=True

time: 65.5 us -> 66.3 us (1.012)
  local copies, waits for them, and re-layouts: 1.13 us -> 0.12 us
  other arithmetic: 0.03 us -> 0.93 us
  waiting for transfers between devices: 18 us -> 18.7 us
    unnamed x13 -> x12, local copies, waits for them, and re-layouts: 1.04 us -> 0.03 us
    another operation x1, other arithmetic: 0.03 us -> 0.93 us  [layer(): two = jnp.stack([flipped, across])]
    ppermute x6, waiting for transfers between devices: 14.5 us -> 15.2 us  [shift(): return lax.ppermute(value, 'kv', [(k, k ^ mask) for k in range(groups)])]
where the time goes in v4:
time: 66.3 us; the launch traced here: 66 us
  Pallas kernels  23 us (35%)
  starting transfers between devices  22.5 us (34%)
  waiting for transfers between devices  18.7 us (28%)
  other arithmetic  0.93 us (1%)
  between operations  0.76 us (1%)
    ppermute x6, waiting for transfers between devices, shift(): return lax.ppermute(value, 'kv', [(k, k ^ mask) for k in range(groups)])  15.2 us
    ppermute x6, starting transfers between devices, shift(): return lax.ppermute(value, 'kv', [(k, k ^ mask) for k in range(groups)])  9.86 us
    all_to_all x1, starting transfers between devices, layer(): lax.all_to_all(tokens.reshape(groups, rows, tokens.shape[1]), 'kv', 0, 0,...  8.17 us
    pallas_call x1, Pallas kernels, read(): pl.pallas_call(functools.partial(read_kernel, steps), out_shape=VMEM((row...  7.38 us
    pallas_call x1, Pallas kernels, commit(): pl.pallas_call(functools.partial(commit_kernel, steps), out_shape=pltpu.H...  7.14 us
    pallas_call x1, Pallas kernels, recall(): pl.pallas_call(functools.partial(recall_kernel, steps), out_shape=(pltpu....  5.95 us
    all_to_all x1, starting transfers between devices, layer(): lax.all_to_all(packed, 'kv', 0, 0, axis_index_groups=members, tiled=True)  4.35 us
    ppermute x1, waiting for transfers between devices, layer(): other = lax.ppermute(send, 'tp', swap)  1.9 us
  transfers between devices with their start and end apart: 9, of which 5 were waited for; matrix products, arithmetic and copies ran while one was open for 2% of the time, Pallas kernels for 31%

profile of v4, /device:TPU:0, one launch (start us, length us, event | category | flops | bytes accessed | tf_op | source)
XLA Modules:
  0.0 66.0 jit_solution(16471053861281826658)
XLA Ops:
  0.6 8.2 %all-to-all-start = ((bf16[16,128,128]{2,1,0:T(8,128)(2,1)}), bf16[16,128,128]{2,1,0:T(8,128)(2,1)S(1)}, u32[]{:S(2)}, u32[]{:S(2)}) async-start(bf16[16,128,128]{2,1,0:T(8,128)(2,1)} %bitcast.21), calls=%async_computation | async-start | bytes 1048576 | tf_op jit(solution)/shard_map/all_to_all | solution.py:584
  8.8 3.4 %collective-permute-start.1 = (bf16[512,128]{1,0:T(8,128)(2,1)}, bf16[512,128]{1,0:T(8,128)(2,1)S(1)}, u32[]{:S(2)}, u32[]{:S(2)}) collective-permute-start(bf16[512,128]{1,0:T(8,128)(2,1)} %param.28), channel_id=1, source_target_pairs={{0,16},{2,18},{4,20},{6,22},{8,24},{10,26},{12,28},{14,30},{16,0},... | collective-permute-start | bytes 393224 | tf_op jit(solution)/shard_map/ppermute | solution.py:580
  12.2 8.8 %collective-permute-done.1 = bf16[512,128]{1,0:T(8,128)(2,1)S(1)} collective-permute-done((bf16[512,128]{1,0:T(8,128)(2,1)}, bf16[512,128]{1,0:T(8,128)(2,1)S(1)}, u32[]{:S(2)}, u32[]{:S(2)}) %collective-permute-start.1) | collective-permute-done | bytes 131104 | tf_op jit(solution)/shard_map/ppermute | solution.py:580
  21.0 0.9 %pad_maximum_fusion.refs_2_ = bf16[2,512,128]{2,1,0:T(8,128)(2,1)S(1)} fusion(bf16[1,512,128]{2,1,0:T(8,128)(2,1)S(1)} %bitcast.24, bf16[1,512,128]{2,1,0:T(8,128)(2,1)} %bitcast.23), kind=kLoop, calls=%fused_computation | loop fusion | flops 131072 | bytes 524288 | tf_op jit(solution)/shard_map/stack | solution.py:587
  21.9 2.8 %collective-permute-start.4 = (bf16[2,512,128]{2,1,0:T(8,128)(2,1)S(1)}, bf16[2,512,128]{2,1,0:T(8,128)(2,1)S(1)}, u32[]{:S(2)}, u32[]{:S(2)}) collective-permute-start(bf16[2,512,128]{2,1,0:T(8,128)(2,1)S(1)} %pad_maximum_fusion.refs_2_), channel_id=1, source_target_pairs={{0,6},{2,4},{4,2},{6,0},{8,14},{10,12},{12,10},{14,8},{16,22},{18,... | collective-permute-start | bytes 786440 | tf_op jit(solution)/shard_map/ppermute | solution.py:580
  24.7 0.9 %collective-permute-start.3 = (bf16[2,512,128]{2,1,0:T(8,128)(2,1)S(1)}, bf16[2,512,128]{2,1,0:T(8,128)(2,1)S(1)}, u32[]{:S(2)}, u32[]{:S(2)}) collective-permute-start(bf16[2,512,128]{2,1,0:T(8,128)(2,1)S(1)} %pad_maximum_fusion.refs_2_), channel_id=1, source_target_pairs={{0,4},{2,6},{4,0},{6,2},{8,12},{10,14},{12,8},{14,10},{16,20},{18,... | collective-permute-start | bytes 786440 | tf_op jit(solution)/shard_map/ppermute | solution.py:580
  25.5 0.6 collective-permute-start.2
  26.1 0.0 copy-start
  26.1 0.0 copy-start.1
  26.1 0.0 copy-start.2
  26.1 0.0 copy-start.3
  26.1 0.0 copy-start.4
  26.1 6.0 %recall.1 = (bf16[4,32,128,128]{3,2,1,0:T(8,128)(2,1)}, bf16[128,512]{1,0:T(8,128)(2,1)S(1)}, bf16[128,512]{1,0:T(8,128)(2,1)S(1)}, f32[128,512]{1,0:T(8,128)S(1)}) custom-call(f32[32,4,128,128]{3,2,1,0:T(8,128)} %state_ref.1, bf16[32,4,4,128]{3,2,1,0:T(4,128)(2,1)} %keys_ref.1, bf16[32,4,4,128]{3,2,1,0:T(4,128)(2,1)} %values_ref.1, f32[4,4,32]{2,1,0:T(4,128)} %bitcast.25, ...), custom_call_target="tpu_custom_call" | custom-call | tf_op jit(solution)/shard_map/recall/pallas_call | solution.py:210
  32.1 0.0 all-to-all-done.tokens_ref
  32.1 0.0 copy-done
  32.1 0.0 copy-done.1
  32.1 0.0 copy-done.2
  32.1 0.0 copy-done.3
  32.1 0.0 copy-done.4
  32.1 7.4 %read.1.refs_0_ = bf16[128,512]{1,0:T(8,128)(2,1)S(1)} custom-call(s32[1]{0:T(128)} %bitcast.2.core_ref, bf16[16,128,128]{2,1,0:T(8,128)(2,1)S(1)} %all-to-all-done.tokens_ref, f32[16,128]{1,0:T(8,128)S(1)} %bitcast.18, bf16[2048,512]{1,0:T(8,128)(2,1)} %query_ref.1, bf16[2048,512]{1,0:T(8,128)(2,1)} %key_ref.1, bf16[2048,512]{1,0:T(8,128)(2,1)} %value_ref.1, ...), custom_call_target="tpu_custom_call" | custom-call | tf_op jit(solution)/shard_map/read/pallas_call | solution.py:428
  39.5 0.0 copy-start.5
  39.5 1.1 %collective-permute-start = (bf16[128,512]{1,0:T(8,128)(2,1)S(1)}, bf16[128,512]{1,0:T(8,128)(2,1)S(1)}, u32[]{:S(2)}, u32[]{:S(2)}) collective-permute-start(bf16[128,512]{1,0:T(8,128)(2,1)S(1)} %read.1.refs_0_), channel_id=1, source_target_pairs={{0,8},{2,10},{4,12},{6,14},{8,0},{10,2},{12,4},{14,6},{16,24},{18,... | collective-permute-start | bytes 393224 | tf_op jit(solution)/shard_map/ppermute | solution.py:580
  40.7 0.0 collective-permute-done.4.refs_5_
  40.7 0.0 collective-permute-done.3.refs_4_
  40.7 0.0 collective-permute-done.2.refs_3_
  40.7 3.9 %collective-permute-done.refs_1_ = bf16[128,512]{1,0:T(8,128)(2,1)S(1)} collective-permute-done((bf16[128,512]{1,0:T(8,128)(2,1)S(1)}, bf16[128,512]{1,0:T(8,128)(2,1)S(1)}, u32[]{:S(2)}, u32[]{:S(2)}) %collective-permute-start) | collective-permute-done | bytes 131104 | tf_op jit(solution)/shard_map/ppermute | solution.py:580
  44.6 0.8 %project.1 = (f32[8,128,256]{2,1,0:T(8,128)S(1)}, bf16[8,128,256]{2,1,0:T(8,128)(2,1)S(1)}) custom-call(bf16[128,512]{1,0:T(8,128)(2,1)S(1)} %read.1.refs_0_, bf16[128,512]{1,0:T(8,128)(2,1)S(1)} %collective-permute-done.refs_1_, bf16[2,512,128]{2,1,0:T(8,128)(2,1)S(1)} %pad_maximum_fusion.refs_2_, bf16[2,512,128]{2,1,0:T(8,128)(2,1)S(1)} %collective-permute-done.2.refs_3_, ...), custom_call_target="tpu_custom_call" | custom-call | tf_op jit(solution)/shard_map/project/pallas_call | solution.py:458
  45.4 0.1 collective-permute-start.5
  45.5 1.9 %collective-permute-done.5.other_ref = bf16[8,128,256]{2,1,0:T(8,128)(2,1)S(1)} collective-permute-done((bf16[8,128,256]{2,1,0:T(8,128)(2,1)S(1)}, bf16[8,128,256]{2,1,0:T(8,128)(2,1)S(1)}, u32[]{:S(2)}, u32[]{:S(2)}) %collective-permute-start.5) | collective-permute-done | bytes 524320 | tf_op jit(solution)/shard_map/ppermute | solution.py:617
  47.4 0.2 combine.1
  47.5 1.1 %collective-permute-start.6 = (f32[8,256]{1,0:T(8,128)S(1)}, f32[8,256]{1,0:T(8,128)S(1)}, u32[]{:S(2)}, u32[]{:S(2)}) collective-permute-start(f32[8,256]{1,0:T(8,128)S(1)} %get-tuple-element.17.refs_0_), channel_id=1, source_target_pairs={{0,8},{2,10},{4,12},{6,14},{8,0},{10,2},{12,4},{14,6},{16,24},{18,... | collective-permute-start | bytes 24584 | tf_op jit(solution)/shard_map/ppermute | solution.py:580
  48.7 0.0 copy-done.5
  48.7 0.1 copy.20.gain_ref
  48.8 2.5 %collective-permute-done.6.refs_1_ = f32[8,256]{1,0:T(8,128)S(1)} collective-permute-done((f32[8,256]{1,0:T(8,128)S(1)}, f32[8,256]{1,0:T(8,128)S(1)}, u32[]{:S(2)}, u32[]{:S(2)}) %collective-permute-start.6) | collective-permute-done | bytes 8224 | tf_op jit(solution)/shard_map/ppermute | solution.py:580
  51.3 0.7 %normalize.1 = bf16[8,64,256]{2,1,0:T(8,128)(2,1)} custom-call(s32[1]{0:T(128)S(6)} %add.14.place_ref, f32[8,64,256]{2,1,0:T(8,128)S(1)} %get-tuple-element.16.sum_ref, f32[8,256]{1,0:T(8,128)S(1)} %get-tuple-element.17.refs_0_, f32[8,256]{1,0:T(8,128)S(1)} %collective-permute-done.6.refs_1_), custom_call_target="tpu_custom_call" | custom-call | tf_op jit(solution)/shard_map/normalize/pallas_call | solution.py:510
  52.0 4.4 %all-to-all-start.1 = ((bf16[8,64,256]{2,1,0:T(8,128)(2,1)}), bf16[8,64,256]{2,1,0:T(8,128)(2,1)S(1)}, u32[]{:S(2)}, u32[]{:S(2)}) async-start(bf16[8,64,256]{2,1,0:T(8,128)(2,1)} %normalize.1), calls=%async_computation.1 | async-start | bytes 524288 | tf_op jit(solution)/shard_map/all_to_all | solution.py:621
  56.4 7.1 %commit.1 = f32[32,4,128,128]{3,2,1,0:T(8,128)} custom-call(f32[32,4,128,128]{3,2,1,0:T(8,128)} %state_ref.1, bf16[128,512]{1,0:T(8,128)(2,1)S(1)} %get-tuple-element.11.unit_ref, bf16[128,512]{1,0:T(8,128)(2,1)S(1)} %get-tuple-element.12.writes_ref, f32[128,512]{1,0:T(8,128)S(1)} %get-tuple-element.13.whole_ref), custom_call_target="tpu_custom_call" | custom-call | flops 4000000000 | tf_op jit(solution)/shard_map/commit/pallas_call | solution.py:290
  63.5 1.6 %all-to-all-done.1.value_ref = bf16[8,64,256]{2,1,0:T(8,128)(2,1)S(1)} async-done(((bf16[8,64,256]{2,1,0:T(8,128)(2,1)}), bf16[8,64,256]{2,1,0:T(8,128)(2,1)S(1)}, u32[]{:S(2)}, u32[]{:S(2)}) %all-to-all-start.1) | async-done | bytes 262176 | tf_op jit(solution)/shard_map/all_to_all | solution.py:621
  65.2 0.8 %spread.1 = bf16[64,2048]{1,0:T(8,128)(2,1)} custom-call(s32[1]{0:T(128)} %bitcast.depth_ref, bf16[8,64,256]{2,1,0:T(8,128)(2,1)S(1)} %all-to-all-done.1.value_ref, f32[64,1]{1,0:T(8,128)S(1)} %copy.20.gain_ref), custom_call_target="tpu_custom_call" | custom-call | tf_op jit(solution)/shard_map/spread/pallas_call | solution.py:536
Async XLA Ops:
  0.6 31.5 %all-to-all-start = ((bf16[16,128,128]{2,1,0:T(8,128)(2,1)}), bf16[16,128,128]{2,1,0:T(8,128)(2,1)S(1)}, u32[]{:S(2)}, u32[]{:S(2)}) async-start(bf16[16,128,128]{2,1,0:T(8,128)(2,1)} %bitcast.21), calls=%async_computation | async-start | bytes 1048576 | tf_op jit(solution)/shard_map/all_to_all | solution.py:584
  8.8 12.2 %collective-permute-start.1 = (bf16[512,128]{1,0:T(8,128)(2,1)}, bf16[512,128]{1,0:T(8,128)(2,1)S(1)}, u32[]{:S(2)}, u32[]{:S(2)}) collective-permute-start(bf16[512,128]{1,0:T(8,128)(2,1)} %param.28), channel_id=1, source_target_pairs={{0,16},{2,18},{4,20},{6,22},{8,24},{10,26},{12,28},{14,30},{16,0},... | collective-permute-start | bytes 393224 | tf_op jit(solution)/shard_map/ppermute | solution.py:580
  21.9 18.8 %collective-permute-start.4 = (bf16[2,512,128]{2,1,0:T(8,128)(2,1)S(1)}, bf16[2,512,128]{2,1,0:T(8,128)(2,1)S(1)}, u32[]{:S(2)}, u32[]{:S(2)}) collective-permute-start(bf16[2,512,128]{2,1,0:T(8,128)(2,1)S(1)} %pad_maximum_fusion.refs_2_), channel_id=1, source_target_pairs={{0,6},{2,4},{4,2},{6,0},{8,14},{10,12},{12,10},{14,8},{16,22},{18,... | collective-permute-start | bytes 786440 | tf_op jit(solution)/shard_map/ppermute | solution.py:580
  24.7 16.0 %collective-permute-start.3 = (bf16[2,512,128]{2,1,0:T(8,128)(2,1)S(1)}, bf16[2,512,128]{2,1,0:T(8,128)(2,1)S(1)}, u32[]{:S(2)}, u32[]{:S(2)}) collective-permute-start(bf16[2,512,128]{2,1,0:T(8,128)(2,1)S(1)} %pad_maximum_fusion.refs_2_), channel_id=1, source_target_pairs={{0,4},{2,6},{4,0},{6,2},{8,12},{10,14},{12,8},{14,10},{16,20},{18,... | collective-permute-start | bytes 786440 | tf_op jit(solution)/shard_map/ppermute | solution.py:580
  25.5 15.1 %collective-permute-start.2 = (bf16[2,512,128]{2,1,0:T(8,128)(2,1)S(1)}, bf16[2,512,128]{2,1,0:T(8,128)(2,1)S(1)}, u32[]{:S(2)}, u32[]{:S(2)}) collective-permute-start(bf16[2,512,128]{2,1,0:T(8,128)(2,1)S(1)} %pad_maximum_fusion.refs_2_), channel_id=1, source_target_pairs={{0,2},{2,0},{4,6},{6,4},{8,10},{10,8},{12,14},{14,12},{16,18},{18,... | collective-permute-start | bytes 786440 | tf_op jit(solution)/shard_map/ppermute | solution.py:580
  26.1 6.0 %copy-start = (bf16[2048,8]{0,1:T(8,128)(2,1)S(1)}, bf16[2048,8]{0,1:T(8,128)(2,1)}, u32[]{:S(2)}) copy-start(bf16[2048,8]{0,1:T(8,128)(2,1)} %param.24) | copy-start | bytes 98308
  26.1 6.0 %copy-start.1 = (bf16[2048,8]{0,1:T(8,128)(2,1)S(1)}, bf16[2048,8]{0,1:T(8,128)(2,1)}, u32[]{:S(2)}) copy-start(bf16[2048,8]{0,1:T(8,128)(2,1)} %param.25) | copy-start | bytes 98308
  26.1 6.0 %copy-start.2 = (f32[2048]{0:T(1024)S(1)}, f32[2048]{0:T(1024)}, u32[]{:S(2)}) copy-start(f32[2048]{0:T(1024)} %param.19) | copy-start | bytes 24580
  26.1 6.0 %copy-start.3 = (f32[4]{0:T(128)S(1)}, f32[4]{0:T(128)}, u32[]{:S(2)}) copy-start(f32[4]{0:T(128)} %param.26) | copy-start | bytes 52
  26.1 6.0 %copy-start.4 = (f32[128]{0:T(128)S(1)}, f32[128]{0:T(128)}, u32[]{:S(2)}) copy-start(f32[128]{0:T(128)} %param.27) | copy-start | bytes 1540
  39.5 9.1 %copy-start.5 = (f32[64]{0:T(128)S(1)}, f32[64]{0:T(128)}, u32[]{:S(2)}) copy-start(f32[64]{0:T(128)} %param.29) | copy-start | bytes 772
  39.5 5.0 %collective-permute-start = (bf16[128,512]{1,0:T(8,128)(2,1)S(1)}, bf16[128,512]{1,0:T(8,128)(2,1)S(1)}, u32[]{:S(2)}, u32[]{:S(2)}) collective-permute-start(bf16[128,512]{1,0:T(8,128)(2,1)S(1)} %read.1.refs_0_), channel_id=1, source_target_pairs={{0,8},{2,10},{4,12},{6,14},{8,0},{10,2},{12,4},{14,6},{16,24},{18,... | collective-permute-start | bytes 393224 | tf_op jit(solution)/shard_map/ppermute | solution.py:580
  45.4 2.0 %collective-permute-start.5 = (bf16[8,128,256]{2,1,0:T(8,128)(2,1)S(1)}, bf16[8,128,256]{2,1,0:T(8,128)(2,1)S(1)}, u32[]{:S(2)}, u32[]{:S(2)}) collective-permute-start(bf16[8,128,256]{2,1,0:T(8,128)(2,1)S(1)} %get-tuple-element.15), channel_id=1, source_target_pairs={{0,1},{1,0},{2,3},{3,2},{4,5},{5,4},{6,7},{7,6},{8,9},{9,8},{10,11... | collective-permute-start | bytes 1572872 | tf_op jit(solution)/shard_map/ppermute | solution.py:617
  47.5 3.7 %collective-permute-start.6 = (f32[8,256]{1,0:T(8,128)S(1)}, f32[8,256]{1,0:T(8,128)S(1)}, u32[]{:S(2)}, u32[]{:S(2)}) collective-permute-start(f32[8,256]{1,0:T(8,128)S(1)} %get-tuple-element.17.refs_0_), channel_id=1, source_target_pairs={{0,8},{2,10},{4,12},{6,14},{8,0},{10,2},{12,4},{14,6},{16,24},{18,... | collective-permute-start | bytes 24584 | tf_op jit(solution)/shard_map/ppermute | solution.py:580
  52.0 13.1 %all-to-all-start.1 = ((bf16[8,64,256]{2,1,0:T(8,128)(2,1)}), bf16[8,64,256]{2,1,0:T(8,128)(2,1)S(1)}, u32[]{:S(2)}, u32[]{:S(2)}) async-start(bf16[8,64,256]{2,1,0:T(8,128)(2,1)} %normalize.1), calls=%async_computation.1 | async-start | bytes 524288 | tf_op jit(solution)/shard_map/all_to_all | solution.py:621
